TPU v7x, 32 devices: a whole 2x2x4 slice. The times are simulated.
32 devices in a mesh: sp: 8 (over z, x), tp: 4 (over y, core).
Axes of the slice: x: 2, y: 2, z: 4, core: 2. Of those that a mesh axis runs over, the one named last changes fastest.
Arguments:
- token_grid: bfloat16 [8, 2048, 512], P('sp', 'tp'), may hold values from -6 to 6
- norm_gain: bfloat16 [3, 2048], replicated, may hold values from 0.099609375 to 1.8984375
- w_query: bfloat16 [3, 2048, 2048], P(None, None, 'tp'), may hold values from -0.125 to 0.125
- w_key: bfloat16 [3, 2048, 2048], P(None, None, 'tp'), may hold values from -0.125 to 0.125
- w_value: bfloat16 [3, 2048, 2048], P(None, None, 'tp'), may hold values from -0.125 to 0.125
- w_out: bfloat16 [3, 2048, 2048], P(None, 'tp'), may hold values from -0.5 to 0.5
- rel_bias: float32 [3, 32, 8, 16], P(None, 'tp'), may hold values from -3 to 250
Outputs:
- grid_out: bfloat16 [8, 2048, 512], P('sp', 'tp')
All inputs are finite; a program needn't handle non-finite values.
Results may differ from a plain program's by a relative error of at most 0.024.
Values may be sent and summed in bfloat16 or wider, within the bound.
A program may use at most 128 MiB of HBM per device.

v0:
```python
import functools

import jax
import jax.numpy as jnp
from jax import lax
from jax.experimental import pallas as pl
from jax.experimental.pallas import tpu as pltpu
from jax.sharding import PartitionSpec as P

HEAD_DIM = 64
WIN_R = 8
WIN_C = 16
EPS = 1e-06
LANES = 128
NEG = -1e30


def attention_kernel(rows, cols, q_ref, k_ref, v_ref, kh_ref, vh_ref, base_ref, o_ref, tile_ref):
    pack = LANES // cols
    n_slots = min(rows, pack + WIN_R - 1)
    half_r = WIN_R // 2
    span = cols + WIN_C
    lane = lax.broadcasted_iota(jnp.int32, (8, LANES), 1)
    lane_q = lax.broadcasted_iota(jnp.int32, (LANES, LANES), 1)
    v_main = v_ref[...].T
    v_halo = vh_ref[...].T
    neg = jnp.full((8, LANES), NEG, jnp.float32)
    outs = [[] for _ in range(rows * cols // LANES)]
    for head in range(LANES // HEAD_DIM):
        for p in range(pack):
            own = (lane >= p * cols) & (lane < (p + 1) * cols)
            for slot in range(WIN_R):
                e = (slot + p) % rows
                start = jnp.broadcast_to(base_ref[head, slot : slot + 1, :], (8, LANES))
                start = pltpu.roll(start, 0, 1, stride=1, stride_axis=0)
                for blk in range(span // 8):
                    shift = (p * cols + 8 * blk) % LANES
                    moved = pltpu.roll(start, shift, 1) if shift else start
                    at = blk - 1 if 1 <= blk <= cols // 8 else (cols // 8 if blk == 0 else blk)
                    where = pl.ds(e * span + 8 * at, 8)
                    rest = neg if p == 0 and rows == WIN_R else tile_ref[where, :]
                    tile_ref[where, :] = jnp.where(own, moved, rest)
        for group in range(rows * cols // LANES):
            key_rows = [r for r in range(rows) if (r - group * pack + half_r) % rows < n_slots]
            q = q_ref[group * LANES : (group + 1) * LANES, :]
            mine = (lane_q >= head * HEAD_DIM) & (lane_q < (head + 1) * HEAD_DIM)
            q = jnp.where(mine, q, jnp.zeros_like(q))
            s_list = []
            contract = (((1,), (1,)), ((), ()))
            if len(key_rows) == rows:
                s_main = lax.dot_general(k_ref[...], q, contract, preferred_element_type=jnp.float32)
                s_halo = lax.dot_general(kh_ref[...], q, contract, preferred_element_type=jnp.float32)
            main_list = []
            halo_list = []
            for r in key_rows:
                e = (r - group * pack + half_r) % rows
                if len(key_rows) == rows:
                    main = s_main[r * cols : (r + 1) * cols]
                    halo = s_halo[r * WIN_C : (r + 1) * WIN_C]
                else:
                    main = lax.dot_general(
                        k_ref[r * cols : (r + 1) * cols, :], q, contract, preferred_element_type=jnp.float32
                    )
                    halo = lax.dot_general(
                        kh_ref[r * WIN_C : (r + 1) * WIN_C, :], q, contract, preferred_element_type=jnp.float32
                    )
                main_list.append(main + tile_ref[e * span : e * span + cols, :])
                halo_list.append(halo + tile_ref[e * span + cols : (e + 1) * span, :])
            main = jnp.concatenate(main_list, axis=0)
            halo = jnp.concatenate(halo_list, axis=0)
            top = jnp.maximum(jnp.max(main, axis=0, keepdims=True), jnp.max(halo, axis=0, keepdims=True))
            main = jnp.exp(main - top)
            halo = jnp.exp(halo - top)
            total = jnp.sum(main, axis=0, keepdims=True) + jnp.sum(halo, axis=0, keepdims=True)
            main = main.astype(jnp.bfloat16)
            halo = halo.astype(jnp.bfloat16)
            lo = head * HEAD_DIM
            if len(key_rows) == rows:
                vm = v_main[lo : lo + HEAD_DIM]
                vh = v_halo[lo : lo + HEAD_DIM]
            else:
                vm = jnp.concatenate([v_main[lo : lo + HEAD_DIM, r * cols : (r + 1) * cols] for r in key_rows], axis=1)
                vh = jnp.concatenate(
                    [v_halo[lo : lo + HEAD_DIM, r * WIN_C : (r + 1) * WIN_C] for r in key_rows], axis=1
                )
            mixed = jnp.dot(vm, main, preferred_element_type=jnp.float32)
            mixed = mixed + jnp.dot(vh, halo, preferred_element_type=jnp.float32)
            outs[group].append(mixed / total)
    for group in range(rows * cols // LANES):
        both = jnp.concatenate(outs[group], axis=0)
        o_ref[group * LANES : (group + 1) * LANES, :] = both.T.astype(o_ref.dtype)


def attention_kernel_init(rows, cols, *refs):
    tile_ref = refs[-1]
    tile_ref[...] = jnp.full(tile_ref.shape, NEG, jnp.float32)
    attention_kernel(rows, cols, *refs)


def attention(queries, keys, values, halo, base, rows, cols):
    tokens, channels = queries.shape
    n_slots = min(rows, LANES // cols + WIN_R - 1)
    pairs = channels // LANES
    per = LANES // HEAD_DIM
    side = halo.shape[0]
    kernel = attention_kernel if rows == WIN_R else attention_kernel_init
    return pl.pallas_call(
        functools.partial(kernel, rows, cols),
        grid=(pairs,),
        out_shape=jax.ShapeDtypeStruct((tokens, channels), jnp.bfloat16),
        in_specs=[
            pl.BlockSpec((tokens, LANES), lambda i: (0, i)),
            pl.BlockSpec((tokens, LANES), lambda i: (0, i)),
            pl.BlockSpec((tokens, LANES), lambda i: (0, i)),
            pl.BlockSpec((side, LANES), lambda i: (0, i)),
            pl.BlockSpec((side, LANES), lambda i: (0, i + pairs)),
            pl.BlockSpec((per, WIN_R, LANES), lambda i: (i, 0, 0)),
        ],
        out_specs=pl.BlockSpec((tokens, LANES), lambda i: (0, i)),
        scratch_shapes=[pltpu.VMEM((n_slots * (cols + WIN_C), LANES), jnp.float32)],
        compiler_params=pltpu.CompilerParams(vmem_limit_bytes=48 * 1024 * 1024),
        name="window_attention",
    )(queries, keys, values, halo, halo, base)


def body(token_grid, norm_gain, w_query, w_key, w_value, w_out, rel_bias):
    n = lax.axis_size("sp")
    rows_dev, channels, columns = token_grid.shape
    rows = rows_dev * n
    cols = columns // n
    tokens = rows * cols
    width = norm_gain.shape[1]
    factor = HEAD_DIM ** (-0.5)
    half_c = WIN_C // 2
    base = jnp.concatenate(
        [
            rel_bias[..., :1],
            jnp.full(rel_bias.shape[:-1] + (LANES - WIN_C,), NEG, jnp.float32),
            jnp.flip(rel_bias[..., 1:], axis=-1),
        ],
        axis=-1,
    )
    turned = jnp.transpose(token_grid, (2, 0, 1)).reshape(columns, rows_dev * channels)
    current = lax.all_to_all(turned, "sp", split_axis=0, concat_axis=0, tiled=True)
    to_right = [(i, (i + 1) % n) for i in range(n)]
    to_left = [(i, (i - 1) % n) for i in range(n)]
    for layer in range(norm_gain.shape[0]):
        gain = norm_gain[layer].astype(jnp.float32)
        raw = lax.all_gather(current, "tp", axis=1, tiled=True).astype(jnp.float32)
        scaled = (raw * gain[None, :]).astype(jnp.bfloat16)
        inverse = lax.rsqrt(jnp.sum(raw * raw, axis=1, keepdims=True) / width + EPS)

        def project(weight, scale=1.0):
            product = jnp.dot(scaled, weight[layer], preferred_element_type=jnp.float32)
            return (product * inverse).astype(jnp.bfloat16) * jnp.bfloat16(scale)

        keys = project(w_key)
        values = project(w_value)
        keyval = jnp.concatenate([keys, values], axis=1).reshape(rows, cols, 2 * channels)
        left = lax.ppermute(keyval[:, cols - half_c :], "sp", to_right)
        right = lax.ppermute(keyval[:, :half_c], "sp", to_left)
        queries = project(w_query, factor)
        halo = jnp.concatenate([left, right], axis=1).reshape(rows * WIN_C, 2 * channels)
        mixed = attention(queries, keys, values, halo, base[layer], rows, cols)
        partial = jnp.dot(mixed, w_out[layer], preferred_element_type=jnp.float32).astype(jnp.bfloat16)
        update = lax.psum_scatter(partial, "tp", scatter_dimension=1, tiled=True)
        current = (current.astype(jnp.float32) + update.astype(jnp.float32)).astype(jnp.bfloat16)
    back = lax.all_to_all(current, "sp", split_axis=0, concat_axis=0, tiled=True)
    return jnp.transpose(back.reshape(columns, rows_dev, channels), (1, 2, 0))


def solution(mesh):
    in_specs = (
        P("sp", "tp", None),
        P(),
        P(None, None, "tp"),
        P(None, None, "tp"),
        P(None, None, "tp"),
        P(None, "tp", None),
        P(None, "tp", None, None),
    )
    out_specs = P("sp", "tp", None)
    return jax.shard_map(body, mesh=mesh, in_specs=in_specs, out_specs=out_specs, check_vma=False)
```

profile of v0, /device:TPU:0, one launch (start us, length us, event | category | flops | bytes accessed | tf_op | source)
XLA Modules:
  0.0 320.6 jit_solution(14276262111966332749)
XLA Ops:
  7.8 21.7 %all_to_all.21 = bf16[8,64,512]{2,1,0:T(8,128)(2,1)} all-to-all(bf16[8,64,512]{2,1,0:T(8,128)(2,1)S(1)} %bitcast.115), channel_id=1, replica_groups=mesh['sp'=8,'tp'=4] {'sp'}, dimensions={0} | all-to-all | bytes 1048576 | tf_op jit(solution)/shard_map/all_to_all | solution.py:144
  30.1 21.3 %all-gather.4.cloned.1.call-done = bf16[512,2048]{1,0:T(8,128)(2,1)} async-done(((bf16[512,512]{1,0:T(8,128)(2,1)}), bf16[512,2048]{1,0:T(8,128)(2,1)}) %all-gather.4.cloned.1.call-update) | async-done | bytes 2097168 | tf_op jit(solution)/shard_map/all_gather | solution.py:149
  53.6 2.8 fusion.128.k_ref
  59.4 4.3 %collective-permute-start.1 = (bf16[8,8,1024]{2,1,0:T(8,128)(2,1)S(1)}, bf16[8,8,1024]{2,1,0:T(8,128)(2,1)S(1)}, u32[]{:S(2)}, u32[]{:S(2)}) collective-permute-start(bf16[8,8,1024]{2,1,0:T(8,128)(2,1)S(1)} %get-tuple-element.10), channel_id=1, source_target_pairs={{0,28},{4,0},{8,4},{12,8},{16,12},{20,16},{24,20},{28,24},{1,29},{... | collective-permute-start | bytes 393224 | tf_op jit(solution)/shard_map/ppermute | solution.py:161
  66.9 4.9 %collective-permute-done = bf16[8,8,1024]{2,1,0:T(8,128)(2,1)S(1)} collective-permute-done((bf16[8,8,1024]{2,1,0:T(8,128)(2,1)S(1)}, bf16[8,8,1024]{2,1,0:T(8,128)(2,1)S(1)}, u32[]{:S(2)}, u32[]{:S(2)}) %collective-permute-start) | collective-permute-done | bytes 131104 | tf_op jit(solution)/shard_map/ppermute | solution.py:160
  71.8 11.3 %window_attention.3 = bf16[512,512]{1,0:T(8,128)(2,1)S(1)} custom-call(bf16[512,512]{1,0:T(8,128)(2,1)S(1)} %fusion.138.q_ref, bf16[512,512]{1,0:T(8,128)(2,1)S(1)} %fusion.128.k_ref, bf16[512,512]{1,0:T(8,128)(2,1)S(1)} %fusion.123.v_ref, bf16[128,1024]{1,0:T(8,128)(2,1)S(1)} %bitcast.108, bf16[128,1024]{1,0:T(8,128)(2,1)S(1)} %bitcast.109, ...), custom_call_target="tpu_custom_call" | custom-call | tf_op jit(solution)/shard_map/window_attention/pallas_call | solution.py:107
  83.1 4.2 %convolution_convert_fusion.2 = bf16[512,2048]{1,0:T(8,128)(2,1)} fusion(bf16[512,512]{1,0:T(8,128)(2,1)S(1)} %window_attention.3, bf16[3,512,2048]{2,1,0:T(8,128)(2,1)} %param.12), kind=kOutput, calls=%fused_computation.14 | convolution fusion | flops 1074790400 | bytes 4718592 | tf_op jit(solution)/shard_map/dot_general | solution.py:165
  87.3 27.7 %reduce-scatter.4.cloned.1.call-done = bf16[512,512]{1,0:T(8,128)(2,1)} async-done(((bf16[512,2048]{1,0:T(8,128)(2,1)}), bf16[512,512]{1,0:T(8,128)(2,1)}) %reduce-scatter.4.cloned.1.call-update) | async-done | bytes 524304 | tf_op jit(solution)/shard_map/reduce_scatter | solution.py:166
  117.1 22.6 %all-gather.6.cloned.1.call-done = bf16[512,2048]{1,0:T(8,128)(2,1)} async-done(((bf16[512,512]{1,0:T(8,128)(2,1)}), bf16[512,2048]{1,0:T(8,128)(2,1)}) %all-gather.6.cloned.1.call-update) | async-done | bytes 2097168 | tf_op jit(solution)/shard_map/all_gather | solution.py:149
  142.0 2.8 fusion.113.k_ref
  144.9 2.9 fusion.108.v_ref
  147.9 4.3 %collective-permute-start.3 = (bf16[8,8,1024]{2,1,0:T(8,128)(2,1)S(1)}, bf16[8,8,1024]{2,1,0:T(8,128)(2,1)S(1)}, u32[]{:S(2)}, u32[]{:S(2)}) collective-permute-start(bf16[8,8,1024]{2,1,0:T(8,128)(2,1)S(1)} %get-tuple-element.8), channel_id=1, source_target_pairs={{0,28},{4,0},{8,4},{12,8},{16,12},{20,16},{24,20},{28,24},{1,29},{... | collective-permute-start | bytes 393224 | tf_op jit(solution)/shard_map/ppermute | solution.py:161
  155.3 4.9 %collective-permute-done.2 = bf16[8,8,1024]{2,1,0:T(8,128)(2,1)S(1)} collective-permute-done((bf16[8,8,1024]{2,1,0:T(8,128)(2,1)S(1)}, bf16[8,8,1024]{2,1,0:T(8,128)(2,1)S(1)}, u32[]{:S(2)}, u32[]{:S(2)}) %collective-permute-start.2) | collective-permute-done | bytes 131104 | tf_op jit(solution)/shard_map/ppermute | solution.py:160
  160.2 11.3 %window_attention.4 = bf16[512,512]{1,0:T(8,128)(2,1)S(1)} custom-call(bf16[512,512]{1,0:T(8,128)(2,1)S(1)} %fusion.143.q_ref, bf16[512,512]{1,0:T(8,128)(2,1)S(1)} %fusion.113.k_ref, bf16[512,512]{1,0:T(8,128)(2,1)S(1)} %fusion.108.v_ref, bf16[128,1024]{1,0:T(8,128)(2,1)S(1)} %bitcast.110, bf16[128,1024]{1,0:T(8,128)(2,1)S(1)} %bitcast.111, ...), custom_call_target="tpu_custom_call" | custom-call | tf_op jit(solution)/shard_map/window_attention/pallas_call | solution.py:107
  171.5 4.2 %convolution_convert_fusion.1 = bf16[512,2048]{1,0:T(8,128)(2,1)} fusion(bf16[512,512]{1,0:T(8,128)(2,1)S(1)} %window_attention.4, bf16[3,512,2048]{2,1,0:T(8,128)(2,1)} %param.12), kind=kOutput, calls=%fused_computation.13 | convolution fusion | flops 1074790400 | bytes 4718592 | tf_op jit(solution)/shard_map/dot_general | solution.py:165
  175.8 27.7 %reduce-scatter.6.cloned.1.call-done = bf16[512,512]{1,0:T(8,128)(2,1)} async-done(((bf16[512,2048]{1,0:T(8,128)(2,1)}), bf16[512,512]{1,0:T(8,128)(2,1)}) %reduce-scatter.6.cloned.1.call-update) | async-done | bytes 524304 | tf_op jit(solution)/shard_map/reduce_scatter | solution.py:166
  205.5 22.7 %all-gather.8.cloned.1.call-done = bf16[512,2048]{1,0:T(8,128)(2,1)} async-done(((bf16[512,512]{1,0:T(8,128)(2,1)}), bf16[512,2048]{1,0:T(8,128)(2,1)}) %all-gather.8.cloned.1.call-update) | async-done | bytes 2097168 | tf_op jit(solution)/shard_map/all_gather | solution.py:149
  230.4 2.8 fusion.98.k_ref
  236.3 4.3 %collective-permute-start.5 = (bf16[8,8,1024]{2,1,0:T(8,128)(2,1)S(1)}, bf16[8,8,1024]{2,1,0:T(8,128)(2,1)S(1)}, u32[]{:S(2)}, u32[]{:S(2)}) collective-permute-start(bf16[8,8,1024]{2,1,0:T(8,128)(2,1)S(1)} %get-tuple-element.6), channel_id=1, source_target_pairs={{0,28},{4,0},{8,4},{12,8},{16,12},{20,16},{24,20},{28,24},{1,29},{... | collective-permute-start | bytes 393224 | tf_op jit(solution)/shard_map/ppermute | solution.py:161
  243.7 4.9 %collective-permute-done.4 = bf16[8,8,1024]{2,1,0:T(8,128)(2,1)S(1)} collective-permute-done((bf16[8,8,1024]{2,1,0:T(8,128)(2,1)S(1)}, bf16[8,8,1024]{2,1,0:T(8,128)(2,1)S(1)}, u32[]{:S(2)}, u32[]{:S(2)}) %collective-permute-start.4) | collective-permute-done | bytes 131104 | tf_op jit(solution)/shard_map/ppermute | solution.py:160
  248.6 11.3 %window_attention.5 = bf16[512,512]{1,0:T(8,128)(2,1)S(1)} custom-call(bf16[512,512]{1,0:T(8,128)(2,1)S(1)} %fusion.148.q_ref, bf16[512,512]{1,0:T(8,128)(2,1)S(1)} %fusion.98.k_ref, bf16[512,512]{1,0:T(8,128)(2,1)S(1)} %fusion.93.v_ref, bf16[128,1024]{1,0:T(8,128)(2,1)S(1)} %bitcast.106, bf16[128,1024]{1,0:T(8,128)(2,1)S(1)} %bitcast.107, ...), custom_call_target="tpu_custom_call" | custom-call | tf_op jit(solution)/shard_map/window_attention/pallas_call | solution.py:107
  259.9 4.2 %convolution_convert_fusion = bf16[512,2048]{1,0:T(8,128)(2,1)} fusion(bf16[512,512]{1,0:T(8,128)(2,1)S(1)} %window_attention.5, bf16[3,512,2048]{2,1,0:T(8,128)(2,1)} %param.12), kind=kOutput, calls=%fused_computation.12 | convolution fusion | flops 1074790400 | bytes 4718592 | tf_op jit(solution)/shard_map/dot_general | solution.py:165
  264.1 27.8 %reduce-scatter.8.cloned.1.call-done = bf16[512,512]{1,0:T(8,128)(2,1)} async-done(((bf16[512,2048]{1,0:T(8,128)(2,1)}), bf16[512,512]{1,0:T(8,128)(2,1)}) %reduce-scatter.8.cloned.1.call-update) | async-done | bytes 524304 | tf_op jit(solution)/shard_map/reduce_scatter | solution.py:166
  293.1 19.7 %all_to_all.22 = bf16[8,64,512]{2,1,0:T(8,128)(2,1)S(1)} all-to-all(bf16[8,64,512]{2,1,0:T(8,128)(2,1)S(1)} %bitcast.113), channel_id=1, replica_groups=mesh['sp'=8,'tp'=4] {'sp'}, dimensions={0} | all-to-all | bytes 1048576 | tf_op jit(solution)/shard_map/all_to_all | solution.py:168
  (66 shorter events, 30.4 us)
Async XLA Ops:
  6.5 23.1 %copy-start.6 = (f32[3,8,8,16]{3,2,1,0:T(8,128)S(1)}, f32[3,8,8,16]{3,2,1,0:T(8,128)}, u32[]{:S(2)}) copy-start(f32[3,8,8,16]{3,2,1,0:T(8,128)} %param.13) | copy-start | bytes 36868
  6.5 23.5 %copy-start.7 = (bf16[3,2048]{1,0:T(4,128)(2,1)S(1)}, bf16[3,2048]{1,0:T(4,128)(2,1)}, u32[]{:S(2)}) copy-start(bf16[3,2048]{1,0:T(4,128)(2,1)} %param.8) | copy-start | bytes 36868
  6.5 44.8 %all-gather.4.cloned.1.call-start = ((), (), s32[]{:S(2)}) async-start(), calls=%async_computation.5 | async-start | bytes 2621440 | tf_op jit(solution)/shard_map/all_gather | solution.py:149
  29.6 85.5 %reduce-scatter.4.cloned.1.call-start = ((), (), s32[]{:S(2)}) async-start(), calls=%async_computation.6 | async-start | bytes 2621440 | tf_op jit(solution)/shard_map/reduce_scatter | solution.py:166
  51.3 2.2 copy-start.3
  59.4 7.4 %collective-permute-start.1 = (bf16[8,8,1024]{2,1,0:T(8,128)(2,1)S(1)}, bf16[8,8,1024]{2,1,0:T(8,128)(2,1)S(1)}, u32[]{:S(2)}, u32[]{:S(2)}) collective-permute-start(bf16[8,8,1024]{2,1,0:T(8,128)(2,1)S(1)} %get-tuple-element.10), channel_id=1, source_target_pairs={{0,28},{4,0},{8,4},{12,8},{16,12},{20,16},{24,20},{28,24},{1,29},{... | collective-permute-start | bytes 393224 | tf_op jit(solution)/shard_map/ppermute | solution.py:161
  63.7 8.0 %collective-permute-start = (bf16[8,8,1024]{2,1,0:T(8,128)(2,1)S(1)}, bf16[8,8,1024]{2,1,0:T(8,128)(2,1)S(1)}, u32[]{:S(2)}, u32[]{:S(2)}) collective-permute-start(bf16[8,8,1024]{2,1,0:T(8,128)(2,1)S(1)} %get-tuple-element.9), channel_id=1, source_target_pairs={{0,4},{4,8},{8,12},{12,16},{16,20},{20,24},{24,28},{28,0},{1,5},{5... | collective-permute-start | bytes 393224 | tf_op jit(solution)/shard_map/ppermute | solution.py:160
  87.3 27.8 %copy-start.2 = (bf16[8,64,512]{2,1,0:T(8,128)(2,1)S(1)}, bf16[8,64,512]{2,1,0:T(8,128)(2,1)}, u32[]{:S(2)}) copy-start(bf16[8,64,512]{2,1,0:T(8,128)(2,1)} %all_to_all.21) | copy-start | bytes 1572868
  87.3 52.5 %all-gather.6.cloned.1.call-start = ((), (), s32[]{:S(2)}) async-start(), calls=%async_computation.7 | async-start | bytes 2621440 | tf_op jit(solution)/shard_map/all_gather | solution.py:149
  117.1 86.4 %reduce-scatter.6.cloned.1.call-start = ((), (), s32[]{:S(2)}) async-start(), calls=%async_computation.8 | async-start | bytes 2621440 | tf_op jit(solution)/shard_map/reduce_scatter | solution.py:166
  139.8 2.2 copy-start.5
  147.9 7.4 %collective-permute-start.3 = (bf16[8,8,1024]{2,1,0:T(8,128)(2,1)S(1)}, bf16[8,8,1024]{2,1,0:T(8,128)(2,1)S(1)}, u32[]{:S(2)}, u32[]{:S(2)}) collective-permute-start(bf16[8,8,1024]{2,1,0:T(8,128)(2,1)S(1)} %get-tuple-element.8), channel_id=1, source_target_pairs={{0,28},{4,0},{8,4},{12,8},{16,12},{20,16},{24,20},{28,24},{1,29},{... | collective-permute-start | bytes 393224 | tf_op jit(solution)/shard_map/ppermute | solution.py:161
  152.2 8.0 %collective-permute-start.2 = (bf16[8,8,1024]{2,1,0:T(8,128)(2,1)S(1)}, bf16[8,8,1024]{2,1,0:T(8,128)(2,1)S(1)}, u32[]{:S(2)}, u32[]{:S(2)}) collective-permute-start(bf16[8,8,1024]{2,1,0:T(8,128)(2,1)S(1)} %get-tuple-element.7), channel_id=1, source_target_pairs={{0,4},{4,8},{8,12},{12,16},{16,20},{20,24},{24,28},{28,0},{1,5},{5... | collective-permute-start | bytes 393224 | tf_op jit(solution)/shard_map/ppermute | solution.py:160
  175.7 27.8 %copy-start = (bf16[512,512]{1,0:T(8,128)(2,1)S(1)}, bf16[512,512]{1,0:T(8,128)(2,1)}, u32[]{:S(2)}) copy-start(bf16[512,512]{1,0:T(8,128)(2,1)} %add_convert_fusion.2) | copy-start | bytes 1572868
  175.7 52.5 %all-gather.8.cloned.1.call-start = ((), (), s32[]{:S(2)}) async-start(), calls=%async_computation.9 | async-start | bytes 2621440 | tf_op jit(solution)/shard_map/all_gather | solution.py:149
  205.5 86.4 %reduce-scatter.8.cloned.1.call-start = ((), (), s32[]{:S(2)}) async-start(), calls=%async_computation.10 | async-start | bytes 2621440 | tf_op jit(solution)/shard_map/reduce_scatter | solution.py:166
  228.2 2.2 copy-start.4
  236.3 7.4 %collective-permute-start.5 = (bf16[8,8,1024]{2,1,0:T(8,128)(2,1)S(1)}, bf16[8,8,1024]{2,1,0:T(8,128)(2,1)S(1)}, u32[]{:S(2)}, u32[]{:S(2)}) collective-permute-start(bf16[8,8,1024]{2,1,0:T(8,128)(2,1)S(1)} %get-tuple-element.6), channel_id=1, source_target_pairs={{0,28},{4,0},{8,4},{12,8},{16,12},{20,16},{24,20},{28,24},{1,29},{... | collective-permute-start | bytes 393224 | tf_op jit(solution)/shard_map/ppermute | solution.py:161
  240.6 8.0 %collective-permute-start.4 = (bf16[8,8,1024]{2,1,0:T(8,128)(2,1)S(1)}, bf16[8,8,1024]{2,1,0:T(8,128)(2,1)S(1)}, u32[]{:S(2)}, u32[]{:S(2)}) collective-permute-start(bf16[8,8,1024]{2,1,0:T(8,128)(2,1)S(1)} %get-tuple-element.5), channel_id=1, source_target_pairs={{0,4},{4,8},{8,12},{12,16},{16,20},{20,24},{24,28},{28,0},{1,5},{5... | collective-permute-start | bytes 393224 | tf_op jit(solution)/shard_map/ppermute | solution.py:160
  264.1 27.8 %copy-start.1 = (bf16[512,512]{1,0:T(8,128)(2,1)S(1)}, bf16[512,512]{1,0:T(8,128)(2,1)}, u32[]{:S(2)}) copy-start(bf16[512,512]{1,0:T(8,128)(2,1)} %add_convert_fusion.1) | copy-start | bytes 1572868
Sparse Core Ops, SparseCore 0:
  29.7 21.5 all-gather.3
  87.4 27.6 reduce-scatter.3
  117.2 22.5 all-gather.5
  175.9 27.5 reduce-scatter.5
  205.6 22.5 all-gather.7
  264.3 27.6 reduce-scatter.7
where the time goes:
time: 321 us
  waiting for transfers between devices  165 us (51%)
  blocking collectives  41.4 us (13%)
  matrix products  38.2 us (12%)
  Pallas kernels  33.8 us (11%)
  between operations  13.7 us (4%)
  starting transfers between devices  13.1 us (4%)
  other arithmetic  12.4 us (4%)
    reduce_scatter x3, waiting for transfers between devices, body(): update = lax.psum_scatter(partial, 'tp', scatter_dimension=1, tiled=True)  83.2 us
    all_gather x3, waiting for transfers between devices, body(): raw = lax.all_gather(current, 'tp', axis=1, tiled=True).astype(jnp.float32)  66.6 us
    pallas_call x3, Pallas kernels, attention(): pl.pallas_call(functools.partial(kernel, rows, cols), grid=(pairs,), out_...  33.8 us
    dot_general x9, matrix products, project(): product = jnp.dot(scaled, weight[layer], preferred_element_type=jnp.float32)  25.6 us
    all_to_all x1, blocking collectives, body(): lax.all_to_all(turned, 'sp', split_axis=0, concat_axis=0, tiled=True)  21.7 us
    all_to_all x1, blocking collectives, body(): lax.all_to_all(current, 'sp', split_axis=0, concat_axis=0, tiled=True)  19.7 us
    ppermute x3, waiting for transfers between devices, body(): left = lax.ppermute(keyval[:, cols - half_c:], 'sp', to_right)  14.7 us
    ppermute x3, starting transfers between devices, body(): right = lax.ppermute(keyval[:, :half_c], 'sp', to_left)  12.9 us
  transfers between devices with their start and end apart: 12, of which 12 were waited for; matrix products, arithmetic and copies ran while one was open for 3% of the time, Pallas kernels for 0%

commit v1 on v0

--- a/solution.py
+++ b/solution.py
@@ -13,6 +13,7 @@
 EPS = 1e-06
 LANES = 128
 NEG = -1e30
+MESH = pl.DeviceIdType.MESH
 
 
 def attention_kernel(rows, cols, q_ref, k_ref, v_ref, kh_ref, vh_ref, base_ref, o_ref, tile_ref):
@@ -168,6 +169,358 @@
     back = lax.all_to_all(current, "sp", split_axis=0, concat_axis=0, tiled=True)
     return jnp.transpose(back.reshape(columns, rows_dev, channels), (1, 2, 0))
 
+def mega_kernel(cfg, *refs):
+    layers, n, chunks, ccols, chan, heads, width = cfg
+    (xt, gain, base, wq, wk, wv, wo, out,
+     w_v, wo_v, xg, xin, xo, sc, q_s, kv, mx, rs_s, rs_r, pre, tile,
+     w_sem, wol_sem, wos_sem, wor_sem, in_s, in_r, ags, agr, hs, hr, ms, mr, rss, rsr, out_s, out_r) = refs
+    f32, bf16 = jnp.float32, jnp.bfloat16
+    tok = ccols * WIN_R
+    half = tok // 2
+    sp, tp = lax.axis_index("sp"), lax.axis_index("tp")
+    core, yy = lax.rem(tp, 2), lax.div(tp, 2)
+    partner = yy * 2 + 1 - core
+    ypeer = (1 - yy) * 2 + core
+    diag = (1 - yy) * 2 + 1 - core
+    right, left = lax.rem(sp + 1, n), lax.rem(sp + n - 1, n)
+
+    def remote(src, dst, ssem, rsem, dev):
+        return pltpu.make_async_remote_copy(
+            src_ref=src, dst_ref=dst, send_sem=ssem, recv_sem=rsem, device_id=dev, device_id_type=MESH
+        )
+
+    bar = pltpu.get_barrier_semaphore()
+    for k in range(1, n):
+        pl.semaphore_signal(bar, inc=1, device_id=(lax.rem(sp + k, n), tp), device_id_type=MESH)
+    pl.semaphore_signal(bar, inc=1, device_id=(sp, partner), device_id_type=MESH)
+    pl.semaphore_signal(bar, inc=1, device_id=(sp, ypeer), device_id_type=MESH)
+    pl.semaphore_wait(bar, n + 1)
+
+    first = (1, 2, 3, 0)
+    for i in first:
+        for k in range(1, n):
+            to = lax.rem(sp + k, n)
+            remote(xt.at[to, i], xin.at[i, sp], in_s.at[i], in_r.at[i], (to, tp)).start()
+
+    def weight_copies(l):
+        return [pltpu.make_async_copy(w.at[l], w_v.at[l, m], w_sem.at[l, m]) for m, w in enumerate((wk, wv, wq))]
+
+    def cols_of(c, other):
+        y_of = (1 - yy) if other else yy
+        return pl.ds(pl.multiple_of((y_of * 2 + c) * chan, 128), chan)
+
+    def own_out(l):
+        return [pltpu.make_async_copy(wo.at[l, :, cols_of(core, o)], wo_v.at[l, core, o], wol_sem.at[l, o]) for o in range(2)]
+
+    def partner_out(l):
+        return [
+            remote(wo.at[l, :, cols_of(1 - core, o)], wo_v.at[l, core, o], wos_sem.at[l, o], wor_sem.at[l, o], (sp, partner))
+            for o in range(2)
+        ]
+
+    for l in range(layers):
+        for c in weight_copies(l) + own_out(l) + partner_out(l):
+            c.start()
+
+    def build(at, carry):
+        l, h = lax.div(at, heads), lax.rem(at, heads)
+        b = base[l, h]
+        for qc in range(ccols):
+            tile[l, h, qc * WIN_R : (qc + 1) * WIN_R, :] = pltpu.roll(b, WIN_R * qc, 1) if qc else b
+        return carry
+
+    lax.fori_loop(0, layers * heads, build, 0)
+
+    a = lax.broadcasted_iota(jnp.int32, (tok, tok), 0)
+    b = lax.broadcasted_iota(jnp.int32, (tok, tok), 1)
+    to_cols = (lax.div(a, WIN_R) == lax.rem(b, ccols)) & (lax.rem(a, WIN_R) == lax.div(b, ccols))
+    to_rows = (lax.div(b, WIN_R) == lax.rem(a, ccols)) & (lax.rem(b, WIN_R) == lax.div(a, ccols))
+
+    def ag_copies(l, i):
+        own = xg.at[l, tp, i]
+        return [
+            remote(own, own, ags.at[l, i, 0], agr.at[l, i, 0], (sp, ypeer)),
+            remote(own, own, ags.at[l, i, 1], agr.at[l, i, 1], (sp, partner)),
+        ]
+
+    def relay_copy(l, i):
+        slot = xg.at[l, ypeer, i]
+        return remote(slot, slot, ags.at[l, i, 2], agr.at[l, i, 2], (sp, partner))
+
+    def ag_send(l, i):
+        for c in ag_copies(l, i):
+            c.start()
+
+    def ag_recv(l, i):
+        ag_copies(l, i)[0].wait_recv()
+        relay_copy(l, i).start()
+        ag_copies(l, i)[1].wait_recv()
+        relay_copy(l, i).wait_recv()
+
+    def init(i):
+        xin[i, sp] = xt[sp, i]
+        some = xin.at[i, pl.ds(0, n - 1)]
+        pltpu.make_async_copy(some, some, in_r.at[i]).wait()
+        raw = xin[i].reshape(tok, chan)
+        mat = jnp.where(to_cols, 1.0, 0.0).astype(bf16)
+        xg[0, tp, i] = jnp.dot(mat, raw, preferred_element_type=f32).astype(bf16)
+        ag_send(0, i)
+
+    def halo_copies(l):
+        return [
+            remote(kv.at[l, :, 2 * chunks], kv.at[l, :, 0], hs.at[l, 0], hr.at[l, 0], (right, tp)),
+            remote(kv.at[l, :, 1], kv.at[l, :, 2 * chunks + 1], hs.at[l, 1], hr.at[l, 1], (left, tp)),
+        ]
+
+    def qkv(l, i):
+        ag_recv(l, i)
+        total = jnp.zeros((tok, 1), f32)
+        for s in range(width // chan):
+            raw = xg[l, s, i].astype(f32)
+            total = total + jnp.sum(raw * raw, axis=1, keepdims=True)
+            sc[:, s * chan : (s + 1) * chan] = (raw * gain[l, :, s * chan : (s + 1) * chan]).astype(bf16)
+        inverse = lax.rsqrt(total / width + EPS)
+        x = sc[...]
+        for m in range(2):
+            prod = jnp.dot(x, w_v[l, m], preferred_element_type=f32) * inverse
+            kv[l, m, pl.ds(1 + 2 * i, 2)] = prod.astype(bf16).reshape(2, half, chan)
+        prod = jnp.dot(x, w_v[l, 2], preferred_element_type=f32) * inverse
+        q_s[i] = prod.astype(bf16) * bf16(HEAD_DIM ** (-0.5))
+
+    def mx_copy(l, i):
+        slot = mx.at[l, core, i]
+        return remote(slot, slot, ms.at[l, i], mr.at[l, i], (sp, partner))
+
+    def attend(l, i):
+        lane = lax.broadcasted_iota(jnp.int32, (tok, LANES), 1)
+        ones = jnp.ones((2 * tok, LANES), bf16)
+        for p in range(chan // LANES):
+            at = slice(p * LANES, (p + 1) * LANES)
+            q = q_s[i, :, at]
+            key = kv[l, 0, pl.ds(2 * i, 4), :, at].reshape(2 * tok, LANES)
+            val = kv[l, 1, pl.ds(2 * i, 4), :, at].reshape(2 * tok, LANES)
+            val = jnp.concatenate([val, ones], axis=1)
+            res = []
+            for hh in range(2):
+                mine = (lane >= hh * HEAD_DIM) & (lane < (hh + 1) * HEAD_DIM)
+                qm = jnp.where(mine, q, jnp.zeros_like(q))
+                s = lax.dot_general(qm, key, (((1,), (1,)), ((), ())), preferred_element_type=f32)
+                s = s + tile[l, 2 * p + hh]
+                e = jnp.exp(s - jnp.max(s, axis=1, keepdims=True)).astype(bf16)
+                o = jnp.dot(e, val, preferred_element_type=f32)
+                res.append(o[:, :LANES] / o[:, LANES:])
+            mx[l, core, i, :, at] = jnp.where(lane < HEAD_DIM, res[0], res[1]).astype(bf16)
+        mx_copy(l, i).start()
+
+    def rs_copy(l, i):
+        return remote(rs_s.at[l, i], rs_r.at[l, i], rss.at[l, i], rsr.at[l, i], (sp, ypeer))
+
+    def project(l, i):
+        mx_copy(l, i).wait_recv()
+        a0, a1 = mx[l, 0, i], mx[l, 1, i]
+
+        def part(o):
+            return jnp.dot(a0, wo_v[l, 0, o], preferred_element_type=f32) + jnp.dot(
+                a1, wo_v[l, 1, o], preferred_element_type=f32
+            )
+
+        rs_s[l, i] = part(1).astype(bf16)
+        rs_copy(l, i).start()
+        pre[i] = xg[l, tp, i].astype(f32) + part(0)
+
+    def updated(l, i):
+        rs_copy(l, i).wait_recv()
+        return (pre[i] + rs_r[l, i].astype(f32)).astype(bf16)
+
+    def finish(l, i):
+        xg[l + 1, tp, i] = updated(l, i)
+        ag_send(l + 1, i)
+
+    def out_copy(i, to):
+        return remote(xo.at[i, to], out.at[sp, i], out_s.at[i], out_r.at[i], (to, tp))
+
+    def finish_last(l, i):
+        mat = jnp.where(to_rows, 1.0, 0.0).astype(bf16)
+        rows = jnp.dot(mat, updated(l, i), preferred_element_type=f32).astype(bf16).reshape(n, ccols, chan)
+        xo[i] = rows
+        for k in range(1, n):
+            out_copy(i, lax.rem(sp + k, n)).start()
+        out[sp, i] = xo[i, sp]
+
+    def layer(l, carry):
+        flip = lax.rem(l, 2)
+
+        def at(i):
+            return i + flip * (chunks - 1 - 2 * i)
+
+        p = [at(i) for i in (1, 2, 3, 0)]
+        order = [at(i) for i in (2, 1, 0, 3)]
+        started = l > 0
+        last = l == layers - 1
+
+        def arrive(i):
+            @pl.when(started)
+            def _():
+                finish(l - 1, i)
+
+            @pl.when(jnp.logical_not(started))
+            def _():
+                init(i)
+
+        def leave(i):
+            @pl.when(last)
+            def _():
+                finish_last(l, i)
+
+            @pl.when(jnp.logical_not(last))
+            def _():
+                finish(l, i)
+
+        for c in weight_copies(l):
+            c.wait()
+        qkv(l, p[0])
+        arrive(p[2])
+        qkv(l, p[1])
+        arrive(p[3])
+        qkv(l, p[2])
+        early, late = 0, 1
+
+        @pl.when(flip == 0)
+        def _():
+            halo_copies(l)[0].start()
+
+        @pl.when(flip == 1)
+        def _():
+            halo_copies(l)[1].start()
+
+        attend(l, order[0])
+        for c in own_out(l):
+            c.wait()
+        for c in partner_out(l):
+            c.wait_recv()
+        project(l, order[0])
+        qkv(l, p[3])
+
+        @pl.when(flip == 0)
+        def _():
+            halo_copies(l)[1].start()
+
+        @pl.when(flip == 1)
+        def _():
+            halo_copies(l)[0].start()
+
+        attend(l, order[1])
+        project(l, order[1])
+        leave(order[0])
+
+        @pl.when(flip == 0)
+        def _():
+            halo_copies(l)[0].wait_recv()
+
+        @pl.when(flip == 1)
+        def _():
+            halo_copies(l)[1].wait_recv()
+
+        attend(l, order[2])
+        project(l, order[2])
+        leave(order[1])
+
+        @pl.when(flip == 0)
+        def _():
+            halo_copies(l)[1].wait_recv()
+
+        @pl.when(flip == 1)
+        def _():
+            halo_copies(l)[0].wait_recv()
+
+        attend(l, order[3])
+        project(l, order[3])
+        return carry
+
+    init(first[0])
+    init(first[1])
+    lax.fori_loop(0, layers, layer, 0)
+    flip = (layers - 1) % 2
+    for i in (0, 3):
+        finish_last(layers - 1, chunks - 1 - i if flip else i)
+
+    for i in range(chunks):
+        some = out.at[pl.ds(0, n - 1), i]
+        pltpu.make_async_copy(some, some, out_r.at[i]).wait()
+        some = xo.at[i, pl.ds(0, n - 1)]
+        pltpu.make_async_copy(some, some, out_s.at[i]).wait()
+        some = xt.at[pl.ds(0, n - 1), i]
+        pltpu.make_async_copy(some, some, in_s.at[i]).wait()
+    for l in range(layers):
+        for c in partner_out(l) + halo_copies(l):
+            c.wait_send()
+        for i in range(chunks):
+            for c in ag_copies(l, i) + [relay_copy(l, i), mx_copy(l, i), rs_copy(l, i)]:
+                c.wait_send()
+
+
+def fused_body(token_grid, norm_gain, w_query, w_key, w_value, w_out, rel_bias):
+    n = lax.axis_size("sp")
+    rows_dev, chan, columns = token_grid.shape
+    layers, width = norm_gain.shape
+    heads = rel_bias.shape[1]
+    chunks = columns // n // WIN_C
+    bf16, f32 = jnp.bfloat16, jnp.float32
+    turned = jnp.transpose(token_grid, (0, 2, 1)).reshape(n, chunks, WIN_C, chan)
+    swapped = jnp.swapaxes(rel_bias, 2, 3)
+    half_r = WIN_R // 2
+    rows = [jnp.roll(swapped, r - half_r, axis=3).reshape(layers, heads, LANES) for r in range(WIN_R)]
+    base = jnp.stack(rows, axis=2)
+    base = jnp.concatenate([base, jnp.full_like(base, NEG)], axis=3)
+    tok = WIN_C * WIN_R
+    half = tok // 2
+    cfg = (layers, n, chunks, WIN_C, chan, heads, width)
+    vmem = pl.BlockSpec(memory_space=pltpu.VMEM)
+    hbm = pl.BlockSpec(memory_space=pl.ANY)
+    dma = pltpu.SemaphoreType.DMA
+    out = pl.pallas_call(
+        functools.partial(mega_kernel, cfg),
+        out_shape=jax.ShapeDtypeStruct((n, chunks, WIN_C, chan), bf16),
+        in_specs=[vmem, vmem, vmem, hbm, hbm, hbm, hbm],
+        out_specs=vmem,
+        scratch_shapes=[
+            pltpu.VMEM((layers, 3, width, chan), bf16),
+            pltpu.VMEM((layers, 2, 2, chan, chan), bf16),
+            pltpu.VMEM((layers, width // chan, chunks, tok, chan), bf16),
+            pltpu.VMEM((chunks, n, WIN_C, chan), bf16),
+            pltpu.VMEM((chunks, n, WIN_C, chan), bf16),
+            pltpu.VMEM((tok, width), bf16),
+            pltpu.VMEM((chunks, tok, chan), bf16),
+            pltpu.VMEM((layers, 2, 2 * chunks + 2, half, chan), bf16),
+            pltpu.VMEM((layers, 2, chunks, tok, chan), bf16),
+            pltpu.VMEM((layers, chunks, tok, chan), bf16),
+            pltpu.VMEM((layers, chunks, tok, chan), bf16),
+            pltpu.VMEM((chunks, tok, chan), f32),
+            pltpu.VMEM((layers, heads, tok, 2 * tok), f32),
+            dma((layers, 3)),
+            dma((layers, 2)),
+            dma((layers, 2)),
+            dma((layers, 2)),
+            dma((chunks,)),
+            dma((chunks,)),
+            dma((layers, chunks, 3)),
+            dma((layers, chunks, 3)),
+            dma((layers, 2)),
+            dma((layers, 2)),
+            dma((layers, chunks)),
+            dma((layers, chunks)),
+            dma((layers, chunks)),
+            dma((layers, chunks)),
+            dma((chunks,)),
+            dma((chunks,)),
+        ],
+        compiler_params=pltpu.CompilerParams(
+            collective_id=0, has_side_effects=True, vmem_limit_bytes=60 * 1024 * 1024
+        ),
+        name="grid_attention",
+    )(turned, norm_gain.astype(f32).reshape(layers, 1, width), base, w_query, w_key, w_value, w_out)
+    return jnp.transpose(out.reshape(rows_dev, columns, chan), (0, 2, 1))
+
 
 def solution(mesh):
     in_specs = (
@@ -180,4 +533,12 @@
         P(None, "tp", None, None),
     )
     out_specs = P("sp", "tp", None)
-    return jax.shard_map(body, mesh=mesh, in_specs=in_specs, out_specs=out_specs, check_vma=False)
+    sharded = functools.partial(jax.shard_map, mesh=mesh, in_specs=in_specs, out_specs=out_specs, check_vma=False)
+
+    def run(token_grid, *rest):
+        rows, _, columns = token_grid.shape
+        n = mesh.shape["sp"]
+        whole = rows == n == WIN_R and columns == 4 * WIN_C * n and mesh.shape["tp"] == 4
+        return sharded(fused_body if whole else body)(token_grid, *rest)
+
+    return run

time: 321 us -> 122 us (0.38)
  waiting for transfers between devices: 165 us -> 0 us
  Pallas kernels: 33.8 us -> 107 us
  blocking collectives: 41.4 us -> 0 us
  matrix products: 38.2 us -> 0 us
  between operations: 13.7 us -> 0.15 us
  starting transfers between devices: 13.1 us -> 0 us
  local copies, waits for them, and re-layouts: 2.64 us -> 15 us
  other arithmetic: 12.4 us -> 0.2 us
    reduce_scatter x3 -> x0, waiting for transfers between devices: 83.2 us -> none  [body(): update = lax.psum_scatter(partial, 'tp', scatter_dimension=1, tiled=True)]
    pallas_call x3 -> x1, Pallas kernels: 33.8 us -> 107 us  [fused_body(): pl.pallas_call(functools.partial(mega_kernel, cfg), out_shape=jax.ShapeDt...]
    all_gather x3 -> x0, waiting for transfers between devices: 66.6 us -> none  [body(): raw = lax.all_gather(current, 'tp', axis=1, tiled=True).astype(jnp.float32)]
    all_to_all x2 -> x0, blocking collectives: 41.4 us -> none  [the longest x1 21.7 us: body(): lax.all_to_all(turned, 'sp', split_axis=0, concat_axis=0, tiled=True)]
    dot_general x12 -> x0, matrix products: 38.2 us -> none  [the longest x9 25.6 us: project(): product = jnp.dot(scaled, weight[layer], preferred_element_type=jnp.float32)]
    ppermute x6 -> x0, waiting for transfers between devices: 15.6 us -> none  [the longest x3 14.7 us: body(): left = lax.ppermute(keyval[:, cols - half_c:], 'sp', to_right)]
    ppermute x6 -> x0, starting transfers between devices: 12.9 us -> none  [the longest x3 12.9 us: body(): right = lax.ppermute(keyval[:, :half_c], 'sp', to_left)]
    slice x4 -> x7, local copies, waits for them, and re-layouts: 0.15 us -> 6.91 us  [fused_body(): jnp.roll(swapped, r - half_r, axis=3).reshape(layers, heads, LANES)]
  transfers between devices with their start and end apart: 12 -> 0, of which waited for: 12 -> 0; matrix products, arithmetic and copies ran while one was open for 3% -> 0% of each run, Pallas kernels for 0% -> 0%
where the time goes in v1:
time: 122 us
  Pallas kernels  107 us (88%)
  local copies, waits for them, and re-layouts  15 us (12%)
    pallas_call x1, Pallas kernels, fused_body(): pl.pallas_call(functools.partial(mega_kernel, cfg), out_shape=jax.ShapeDt...  107 us
    slice x7, local copies, waits for them, and re-layouts, fused_body(): jnp.roll(swapped, r - half_r, axis=3).reshape(layers, heads, LANES)  6.91 us

profile of v1, /device:TPU:0, one launch (start us, length us, event | category | flops | bytes accessed | tf_op | source)
XLA Modules:
  0.0 122.0 jit_solution(6112608473239808859)
XLA Ops:
  0.0 1.4 %reshape.16.refs_1_ = f32[3,1,2048]{2,1,0:T(1,128)} reshape(bf16[3,2048]{1,0:T(4,128)(2,1)} %param.8) | data formatting | bytes 36864 | tf_op jit(solution)/shard_map/reshape | solution.py:521
  1.4 1.0 fusion.4
  2.4 1.0 fusion.2
  3.4 1.0 fusion
  4.4 1.0 fusion.6
  5.4 0.1 copy.19
  5.5 0.1 stack_reshape.24
  5.7 1.0 copy.23
  6.7 0.1 stack_reshape.28
  6.8 1.0 fusion.1
  7.8 0.1 copy.20
  8.0 0.1 stack_reshape.25
  8.2 0.1 stack_reshape.31
  8.3 1.0 fusion.3
  9.5 0.1 stack_reshape.26
  9.8 0.1 stack_reshape.30
  9.9 1.0 fusion.5
  11.0 0.1 stack_reshape.27
  11.3 0.1 stack_reshape.29
  11.4 0.2 stack.3
  11.6 0.7 concatenate.38.refs_2_
  12.3 1.0 copy.18
  13.3 106.6 %grid_attention.1 = bf16[8,4,16,512]{3,2,1,0:T(8,128)(2,1)} custom-call(bf16[8,4,16,512]{3,2,1,0:T(8,128)(2,1)} %bitcast.38, f32[3,1,2048]{2,1,0:T(1,128)} %reshape.16.refs_1_, f32[3,8,8,256]{3,2,1,0:T(8,128)} %concatenate.38.refs_2_, bf16[3,2048,512]{2,1,0:T(8,128)(2,1)} %refs_3_.1, bf16[3,2048,512]{2,1,0:T(8,128)(2,1)} %refs_4_.1, ...), custom_call_target="tpu_custom_call" | custom-call | tf_op jit(solution)/shard_map/grid_attention/pallas_call | solution.py:481
  119.9 2.0 %copy.35 = bf16[1,512,512]{1,2,0:T(8,128)(2,1)} copy(bf16[1,512,512]{2,1,0:T(8,128)(2,1)} %bitcast.37) | data formatting | bytes 1048576 | tf_op jit(solution)/shard_map/reshape | solution.py:522
  (11 shorter events, 0.7 us)
Async XLA Ops:
  0.0 12.3 %copy-start = (bf16[1,512,512]{2,1,0:T(8,128)(2,1)S(1)}, bf16[1,512,512]{2,1,0:T(8,128)(2,1)}, u32[]{:S(2)}) copy-start(bf16[1,512,512]{2,1,0:T(8,128)(2,1)} %param.7) | copy-start | bytes 1572868

commit v2 on v1

--- a/solution.py
+++ b/solution.py
@@ -171,8 +171,8 @@
 
 def mega_kernel(cfg, *refs):
     layers, n, chunks, ccols, chan, heads, width = cfg
-    (xt, gain, base, wq, wk, wv, wo, out,
-     w_v, wo_v, xg, xin, xo, sc, q_s, kv, mx, rs_s, rs_r, pre, tile,
+    (xt, gain, bias, wq, wk, wv, wo, out,
+     w_v, wo_v, xg, xin, xo, sc, q_s, kv, mx, rs_s, rs_r, pre, tile, wide,
      w_sem, wol_sem, wos_sem, wor_sem, in_s, in_r, ags, agr, hs, hr, ms, mr, rss, rsr, out_s, out_r) = refs
     f32, bf16 = jnp.float32, jnp.bfloat16
     tok = ccols * WIN_R
@@ -222,9 +222,22 @@
         for c in weight_copies(l) + own_out(l) + partner_out(l):
             c.start()
 
+    spread_at = lax.broadcasted_iota(jnp.int32, (ccols, LANES), 0)
+    spread_to = lax.broadcasted_iota(jnp.int32, (ccols, LANES), 1)
+    spread = jnp.where(lax.div(spread_to, WIN_R) == spread_at, 1.0, 0.0)
+    wide[...] = jnp.dot(bias[...], spread, preferred_element_type=f32, precision=lax.Precision.HIGHEST)
+    query_row = lax.broadcasted_iota(jnp.int32, (WIN_R, LANES), 0)
+    key_row = lax.rem(lax.broadcasted_iota(jnp.int32, (WIN_R, LANES), 1), WIN_R)
+    slot_row = lax.rem(key_row - query_row + WIN_R + WIN_R // 2, WIN_R)
+    outside = jnp.full((WIN_R, LANES), NEG, f32)
+
     def build(at, carry):
         l, h = lax.div(at, heads), lax.rem(at, heads)
-        b = base[l, h]
+        slots = wide[pl.ds(pl.multiple_of(at * WIN_R, WIN_R), WIN_R), :]
+        b = jnp.zeros((WIN_R, LANES), f32)
+        for i in range(WIN_R):
+            b = jnp.where(slot_row == i, slots[i : i + 1, :], b)
+        b = jnp.concatenate([b, outside], axis=1)
         for qc in range(ccols):
             tile[l, h, qc * WIN_R : (qc + 1) * WIN_R, :] = pltpu.roll(b, WIN_R * qc, 1) if qc else b
         return carry
@@ -383,7 +396,6 @@
         qkv(l, p[1])
         arrive(p[3])
         qkv(l, p[2])
-        early, late = 0, 1
 
         @pl.when(flip == 0)
         def _():
@@ -467,11 +479,6 @@
     chunks = columns // n // WIN_C
     bf16, f32 = jnp.bfloat16, jnp.float32
     turned = jnp.transpose(token_grid, (0, 2, 1)).reshape(n, chunks, WIN_C, chan)
-    swapped = jnp.swapaxes(rel_bias, 2, 3)
-    half_r = WIN_R // 2
-    rows = [jnp.roll(swapped, r - half_r, axis=3).reshape(layers, heads, LANES) for r in range(WIN_R)]
-    base = jnp.stack(rows, axis=2)
-    base = jnp.concatenate([base, jnp.full_like(base, NEG)], axis=3)
     tok = WIN_C * WIN_R
     half = tok // 2
     cfg = (layers, n, chunks, WIN_C, chan, heads, width)
@@ -497,6 +504,7 @@
             pltpu.VMEM((layers, chunks, tok, chan), bf16),
             pltpu.VMEM((chunks, tok, chan), f32),
             pltpu.VMEM((layers, heads, tok, 2 * tok), f32),
+            pltpu.VMEM((layers * heads * WIN_R, LANES), f32),
             dma((layers, 3)),
             dma((layers, 2)),
             dma((layers, 2)),
@@ -518,7 +526,7 @@
             collective_id=0, has_side_effects=True, vmem_limit_bytes=60 * 1024 * 1024
         ),
         name="grid_attention",
-    )(turned, norm_gain.astype(f32).reshape(layers, 1, width), base, w_query, w_key, w_value, w_out)
+    )(turned, norm_gain.astype(f32).reshape(layers, 1, width), rel_bias.reshape(-1, WIN_C), w_query, w_key, w_value, w_out)
     return jnp.transpose(out.reshape(rows_dev, columns, chan), (0, 2, 1))
 
 

time: 122 us -> 112 us (0.918)
  local copies, waits for them, and re-layouts: 15 us -> 5.42 us
    slice x7 -> x0, local copies, waits for them, and re-layouts: 6.91 us -> none  [fused_body(): jnp.roll(swapped, r - half_r, axis=3).reshape(layers, heads, LANES)]
    concatenate x8 -> x0, local copies, waits for them, and re-layouts: 1.43 us -> none  [the longest x7 0.73 us: fused_body(): jnp.roll(swapped, r - half_r, axis=3).reshape(layers, heads, LANES)]
where the time goes in v2:
time: 112 us
  Pallas kernels  107 us (96%)
  local copies, waits for them, and re-layouts  5.42 us (5%)
    pallas_call x1, Pallas kernels, fused_body(): pl.pallas_call(functools.partial(mega_kernel, cfg), out_shape=jax.ShapeDt...  107 us

profile of v2, /device:TPU:0, one launch (start us, length us, event | category | flops | bytes accessed | tf_op | source)
XLA Modules:
  0.0 112.1 jit_solution(8567296954814812219)
XLA Ops:
  0.0 1.3 %reshape.20.refs_1_ = f32[3,1,2048]{2,1,0:T(1,128)} reshape(bf16[3,2048]{1,0:T(4,128)(2,1)} %param.8) | data formatting | bytes 36864 | tf_op jit(solution)/shard_map/reshape | solution.py:529
  1.3 2.0 %copy.8 = bf16[1,512,512]{2,1,0:T(8,128)(2,1)} copy(bf16[1,512,512]{1,2,0:T(8,128)(2,1)} %bitcast.7) | data formatting | bytes 1048576 | tf_op jit(solution)/shard_map/transpose | solution.py:481
  3.4 106.6 %grid_attention.1 = bf16[8,4,16,512]{3,2,1,0:T(8,128)(2,1)} custom-call(bf16[8,4,16,512]{3,2,1,0:T(8,128)(2,1)} %bitcast.6, f32[3,1,2048]{2,1,0:T(1,128)} %reshape.20.refs_1_, f32[192,16]{1,0:T(8,128)} %bitcast.8, bf16[3,2048,512]{2,1,0:T(8,128)(2,1)} %refs_3_.1, bf16[3,2048,512]{2,1,0:T(8,128)(2,1)} %refs_4_.1, bf16[3,2048,512]{2,1,0:T(8,128)(2,1)} %refs_5_.1, ...), custom_call_target="tpu_custom_call" | custom-call | tf_op jit(solution)/shard_map/grid_attention/pallas_call | solution.py:488
  110.0 2.0 %copy.9 = bf16[1,512,512]{1,2,0:T(8,128)(2,1)} copy(bf16[1,512,512]{2,1,0:T(8,128)(2,1)} %bitcast.5) | data formatting | bytes 1048576 | tf_op jit(solution)/shard_map/reshape | solution.py:530

commit v3 on v2

--- a/solution.py
+++ b/solution.py
@@ -169,8 +169,101 @@
     back = lax.all_to_all(current, "sp", split_axis=0, concat_axis=0, tiled=True)
     return jnp.transpose(back.reshape(columns, rows_dev, channels), (1, 2, 0))
 
+def unit_pairs(blocks):
+    odd = [(b, (b + 1) % blocks) for b in range(1, blocks, 2)]
+    even = [((b + 1) % blocks, (b + 2) % blocks) for b in range(1, blocks, 2)]
+    return odd, even
+
+
+def plan(layers, blocks, starts, orders):
+    link, hop, near, mixed, halo_link, halo_hop = 2.82, 1.8, 1.45, 1.4, 2.8, 2.2
+    odd, even = unit_pairs(blocks)
+    units = [odd if l % 2 == 0 else even for l in range(layers + 1)]
+    count = len(odd)
+    gathered = [starts] + orders
+
+    def needs(l, i):
+        wanted, sides = set(), []
+        for b in units[l + 1][i]:
+            for near_b in (b - 1, b, b + 1):
+                if 0 <= near_b < blocks:
+                    wanted.update(u for u, pair in enumerate(units[l]) if near_b in pair)
+                else:
+                    sides.append(near_b < 0)
+        return wanted, sides
+
+    now, wire = 0.0, 0.0
+    side_wire = {True: 0.0, False: 0.0}
+    own, across, relayed, done, halo, mx, sums = {}, {}, {}, set(), {}, {}, {}
+    at = {kind: [0] * layers for kind in ("qkv", "attend", "project", "finish", "relay")}
+    first, steps = 0, []
+
+    def send(t, loads=1):
+        nonlocal wire
+        wire = max(t, wire) + loads * link
+        return wire + hop
+
+    while True:
+        ready = []
+        if first < count:
+            ready.append((4.5 + 2.7 * first, 0, "init", 0, starts[first]))
+        for l in range(layers):
+            def step(kind, order):
+                return order[at[kind][l]] if at[kind][l] < count else None
+
+            i = step("finish", orders[l])
+            if (l, i) in sums:
+                ready.append((sums[l, i], 1, "finish", l, i))
+            i = step("relay", gathered[l])
+            if l == 0 and (l, i) in across:
+                ready.append((across[l, i], 2, "relay", l, i))
+            i = step("project", orders[l])
+            if (l, i) in mx:
+                ready.append((mx[l, i], 3, "project", l, i))
+            i = step("attend", orders[l])
+            if i is not None:
+                wanted, sides = needs(l, i)
+                if all((l, u) in done for u in wanted) and all((l, side) in halo for side in sides):
+                    ready.append((max([0.0] + [halo[l, side] for side in sides]), 4, "attend", l, i))
+            i = step("qkv", gathered[l])
+            if (l, i) in relayed:
+                ready.append((max(relayed[l, i], own[l, i]), 5, "qkv", l, i))
+        if not ready:
+            return steps
+        can = [r for r in ready if r[0] <= now]
+        when, _, kind, l, i = min(can, key=lambda r: r[1:]) if can else min(ready)
+        now = max(now, when)
+        steps.append((kind, l, i))
+        if kind == "init":
+            first += 1
+            now += 0.18
+            across[0, i], own[0, i] = send(now), now + near
+            continue
+        at[kind][l] += 1
+        if kind == "relay":
+            relayed[l, i] = now + near
+        elif kind == "qkv":
+            done.add((l, i))
+            for side, edge in ((True, blocks - 1), (False, 0)):
+                if edge in units[l][i]:
+                    side_wire[side] = max(now + 0.75, side_wire[side]) + halo_link
+                    halo[l, side] = side_wire[side] + halo_hop
+            now += 1.02
+        elif kind == "attend":
+            pair = units[l + 1][i]
+            now += 0.64 if pair[0] < pair[1] else 1.0
+            mx[l, i] = now + mixed
+        elif kind == "project":
+            sums[l, i] = send(now + 0.35, 1 if l == layers - 1 else 2)
+            now += 0.65
+        else:
+            now += 0.15
+            if l < layers - 1:
+                relayed[l + 1, i] = own[l + 1, i] = now + near
+
+
 def mega_kernel(cfg, *refs):
-    layers, n, chunks, ccols, chan, heads, width = cfg
+    layers, n, chunks, ccols, chan, heads, width, steps = cfg
     (xt, gain, bias, wq, wk, wv, wo, out,
      w_v, wo_v, xg, xin, xo, sc, q_s, kv, mx, rs_s, rs_r, pre, tile, wide,
      w_sem, wol_sem, wos_sem, wor_sem, in_s, in_r, ags, agr, hs, hr, ms, mr, rss, rsr, out_s, out_r) = refs
@@ -182,7 +275,18 @@
     partner = yy * 2 + 1 - core
     ypeer = (1 - yy) * 2 + core
     diag = (1 - yy) * 2 + 1 - core
-    right, left = lax.rem(sp + 1, n), lax.rem(sp + n - 1, n)
+    deep = n // 2
+
+    def place(dev):
+        z, x = lax.div(dev, 2), lax.rem(dev, 2)
+        return z + x * (n - 1 - 2 * z)
+
+    def holder(at):
+        back = lax.div(at, deep)
+        return 2 * (at + back * (n - 1 - 2 * at)) + back
+
+    mine_at = place(sp)
+    right, left = holder(lax.rem(mine_at + 1, n)), holder(lax.rem(mine_at + n - 1, n))
 
     def remote(src, dst, ssem, rsem, dev):
         return pltpu.make_async_remote_copy(
@@ -196,18 +300,34 @@
     pl.semaphore_signal(bar, inc=1, device_id=(sp, ypeer), device_id_type=MESH)
     pl.semaphore_wait(bar, n + 1)
 
-    first = (1, 2, 3, 0)
-    for i in first:
+    blocks = 2 * chunks
+    odd, even = unit_pairs(blocks)
+    units = [odd if l % 2 == 0 else even for l in range(layers + 1)]
+
+    def sends_in(i):
+        (b0, b1), out = odd[i], []
         for k in range(1, n):
             to = lax.rem(sp + k, n)
-            remote(xt.at[to, i], xin.at[i, sp], in_s.at[i], in_r.at[i], (to, tp)).start()
+            if b1 == b0 + 1:
+                out.append(remote(xt.at[place(to), b0 : b0 + 2], xin.at[i, :, sp], in_s.at[i], in_r.at[i], (to, tp)))
+            else:
+                for j, blk in enumerate((b0, b1)):
+                    out.append(remote(xt.at[place(to), blk], xin.at[i, j, sp], in_s.at[i], in_r.at[i], (to, tp)))
+        return out
+
+    def sent_in(i):
+        some = xin.at[i, :, pl.ds(0, n - 1)]
+        pltpu.make_async_copy(some, some, in_s.at[i]).wait()
+
+    for i in range(2):
+        for c in sends_in(i):
+            c.start()
 
     def weight_copies(l):
         return [pltpu.make_async_copy(w.at[l], w_v.at[l, m], w_sem.at[l, m]) for m, w in enumerate((wk, wv, wq))]
 
-    def cols_of(c, other):
-        y_of = (1 - yy) if other else yy
-        return pl.ds(pl.multiple_of((y_of * 2 + c) * chan, 128), chan)
+    def cols_of(c, o):
+        return pl.ds(pl.multiple_of((o * 2 + c) * chan, 128), chan)
 
     def own_out(l):
         return [pltpu.make_async_copy(wo.at[l, :, cols_of(core, o)], wo_v.at[l, core, o], wol_sem.at[l, o]) for o in range(2)]
@@ -218,9 +338,8 @@
             for o in range(2)
         ]
 
-    for l in range(layers):
-        for c in weight_copies(l) + own_out(l) + partner_out(l):
-            c.start()
+    for c in weight_copies(0) + own_out(0) + partner_out(0):
+        c.start()
 
     spread_at = lax.broadcasted_iota(jnp.int32, (ccols, LANES), 0)
     spread_to = lax.broadcasted_iota(jnp.int32, (ccols, LANES), 1)
@@ -244,10 +363,17 @@
 
     lax.fori_loop(0, layers * heads, build, 0)
 
+    for i in range(2, chunks):
+        sent_in(i - 2)
+        for c in sends_in(i):
+            c.start()
+
     a = lax.broadcasted_iota(jnp.int32, (tok, tok), 0)
     b = lax.broadcasted_iota(jnp.int32, (tok, tok), 1)
-    to_cols = (lax.div(a, WIN_R) == lax.rem(b, ccols)) & (lax.rem(a, WIN_R) == lax.div(b, ccols))
-    to_rows = (lax.div(b, WIN_R) == lax.rem(a, ccols)) & (lax.rem(b, WIN_R) == lax.div(a, ccols))
+    same = lax.div(a, half) == lax.div(b, half)
+    ra, rb = lax.rem(a, half), lax.rem(b, half)
+    swap = same & (lax.div(ra, WIN_R) == lax.rem(rb, WIN_R)) & (lax.rem(ra, WIN_R) == lax.div(rb, WIN_R))
+    swap = jnp.where(swap, 1.0, 0.0).astype(bf16)
 
     def ag_copies(l, i):
         own = xg.at[l, tp, i]
@@ -264,19 +390,30 @@
         for c in ag_copies(l, i):
             c.start()
 
-    def ag_recv(l, i):
+    def relay(l, i):
         ag_copies(l, i)[0].wait_recv()
         relay_copy(l, i).start()
-        ag_copies(l, i)[1].wait_recv()
-        relay_copy(l, i).wait_recv()
+
+    def partner_copies(l, i):
+        slots = [xg.at[l, 2 * o + core, i] for o in range(2)]
+        return [remote(slots[o], slots[o], ags.at[l, i, o], agr.at[l, i, o], (sp, partner)) for o in range(2)]
+
+    def ag_recv(l, i):
+        if l == 0:
+            ag_copies(l, i)[1].wait_recv()
+            relay_copy(l, i).wait_recv()
+        else:
+            for c in partner_copies(l, i):
+                c.wait_recv()
 
     def init(i):
-        xin[i, sp] = xt[sp, i]
-        some = xin.at[i, pl.ds(0, n - 1)]
+        b0, b1 = odd[i]
+        for j, blk in enumerate((b0, b1)):
+            xin[i, j, sp] = xt[mine_at, blk]
+        some = xin.at[i, :, pl.ds(0, n - 1)]
         pltpu.make_async_copy(some, some, in_r.at[i]).wait()
-        raw = xin[i].reshape(tok, chan)
-        mat = jnp.where(to_cols, 1.0, 0.0).astype(bf16)
-        xg[0, tp, i] = jnp.dot(mat, raw, preferred_element_type=f32).astype(bf16)
+        raw = xin[i].astype(f32).reshape(tok, chan).astype(bf16)
+        xg[0, tp, i] = jnp.dot(swap, raw, preferred_element_type=f32).astype(bf16)
         ag_send(0, i)
 
     def halo_copies(l):
@@ -296,37 +433,62 @@
         x = sc[...]
         for m in range(2):
             prod = jnp.dot(x, w_v[l, m], preferred_element_type=f32) * inverse
-            kv[l, m, pl.ds(1 + 2 * i, 2)] = prod.astype(bf16).reshape(2, half, chan)
+            prod = prod.astype(bf16)
+            for j, blk in enumerate(units[l][i]):
+                kv[l, m, 1 + blk] = prod[j * half : (j + 1) * half]
+        if 0 in units[l][i]:
+            halo_copies(l)[1].start()
+        if blocks - 1 in units[l][i]:
+            halo_copies(l)[0].start()
         prod = jnp.dot(x, w_v[l, 2], preferred_element_type=f32) * inverse
-        q_s[i] = prod.astype(bf16) * bf16(HEAD_DIM ** (-0.5))
+        prod = prod.astype(bf16) * bf16(HEAD_DIM ** (-0.5))
+        for j, blk in enumerate(units[l][i]):
+            q_s[blk] = prod[j * half : (j + 1) * half]
 
     def mx_copy(l, i):
         slot = mx.at[l, core, i]
         return remote(slot, slot, ms.at[l, i], mr.at[l, i], (sp, partner))
 
-    def attend(l, i):
-        lane = lax.broadcasted_iota(jnp.int32, (tok, LANES), 1)
+    def window(l, q0, qn, k0, t0, out_at):
+        rows = qn * half
+        lane = lax.broadcasted_iota(jnp.int32, (rows, LANES), 1)
         ones = jnp.ones((2 * tok, LANES), bf16)
         for p in range(chan // LANES):
             at = slice(p * LANES, (p + 1) * LANES)
-            q = q_s[i, :, at]
-            key = kv[l, 0, pl.ds(2 * i, 4), :, at].reshape(2 * tok, LANES)
-            val = kv[l, 1, pl.ds(2 * i, 4), :, at].reshape(2 * tok, LANES)
+            q = q_s[q0 : q0 + qn, :, at].reshape(rows, LANES)
+            key = kv[l, 0, k0 : k0 + 4, :, at].reshape(2 * tok, LANES)
+            val = kv[l, 1, k0 : k0 + 4, :, at].reshape(2 * tok, LANES)
             val = jnp.concatenate([val, ones], axis=1)
             res = []
             for hh in range(2):
                 mine = (lane >= hh * HEAD_DIM) & (lane < (hh + 1) * HEAD_DIM)
                 qm = jnp.where(mine, q, jnp.zeros_like(q))
                 s = lax.dot_general(qm, key, (((1,), (1,)), ((), ())), preferred_element_type=f32)
-                s = s + tile[l, 2 * p + hh]
+                s = s + tile[l, 2 * p + hh, t0 : t0 + rows]
                 e = jnp.exp(s - jnp.max(s, axis=1, keepdims=True)).astype(bf16)
                 o = jnp.dot(e, val, preferred_element_type=f32)
                 res.append(o[:, :LANES] / o[:, LANES:])
-            mx[l, core, i, :, at] = jnp.where(lane < HEAD_DIM, res[0], res[1]).astype(bf16)
+            out_at[:, at] = jnp.where(lane < HEAD_DIM, res[0], res[1]).astype(bf16)
+
+    def attend(l, i):
+        b0, b1 = units[l + 1][i]
+        if b1 == b0 + 1:
+            window(l, b0, 2, b0, 0, mx.at[l, core, i])
+        else:
+            window(l, b0, 1, b0 - 1, half, mx.at[l, core, i, :half])
+            window(l, b1, 1, b1, 0, mx.at[l, core, i, half:])
         mx_copy(l, i).start()
 
-    def rs_copy(l, i):
-        return remote(rs_s.at[l, i], rs_r.at[l, i], rss.at[l, i], rsr.at[l, i], (sp, ypeer))
+    def rs_copy(l, i, o):
+        return remote(rs_s.at[l, i, o], rs_r.at[l, i, o], rss.at[l, i, o], rsr.at[l, i, o], (sp, ypeer))
+
+    def old(l, i, slot):
+        parts = []
+        for blk in units[l + 1][i]:
+            u = [blk in pair for pair in units[l]].index(True)
+            k = units[l][u].index(blk)
+            parts.append(xg[l, slot, u, k * half : (k + 1) * half])
+        return jnp.concatenate(parts, axis=0).astype(f32)
 
     def project(l, i):
         mx_copy(l, i).wait_recv()
@@ -337,137 +499,109 @@
                 a1, wo_v[l, 1, o], preferred_element_type=f32
             )
 
-        rs_s[l, i] = part(1).astype(bf16)
-        rs_copy(l, i).start()
-        pre[i] = xg[l, tp, i].astype(f32) + part(0)
-
-    def updated(l, i):
-        rs_copy(l, i).wait_recv()
-        return (pre[i] + rs_r[l, i].astype(f32)).astype(bf16)
+        if l == layers - 1:
+            rs_s[l, i, 0] = part(1 - yy).astype(bf16)
+            rs_copy(l, i, 0).start()
+            pre[i] = old(l, i, tp) + part(yy)
+        else:
+            for o in range(2):
+                rs_s[l, i, o] = part(o).astype(bf16)
+                rs_copy(l, i, o).start()
+
+    def updated(i):
+        rs_copy(layers - 1, i, 0).wait_recv()
+        return (pre[i] + rs_r[layers - 1, i, 0].astype(f32)).astype(bf16)
 
     def finish(l, i):
-        xg[l + 1, tp, i] = updated(l, i)
-        ag_send(l + 1, i)
-
-    def out_copy(i, to):
-        return remote(xo.at[i, to], out.at[sp, i], out_s.at[i], out_r.at[i], (to, tp))
-
-    def finish_last(l, i):
-        mat = jnp.where(to_rows, 1.0, 0.0).astype(bf16)
-        rows = jnp.dot(mat, updated(l, i), preferred_element_type=f32).astype(bf16).reshape(n, ccols, chan)
-        xo[i] = rows
+        for o in range(2):
+            rs_copy(l, i, o).wait_recv()
+            slot = 2 * o + core
+            both = rs_s[l, i, o].astype(f32) + rs_r[l, i, o].astype(f32)
+            xg[l + 1, slot, i] = (old(l, i, slot) + both).astype(bf16)
+            partner_copies(l + 1, i)[o].start()
+
+    def out_copies(i):
+        (b0, b1), out_list = units[layers][i], []
         for k in range(1, n):
-            out_copy(i, lax.rem(sp + k, n)).start()
-        out[sp, i] = xo[i, sp]
-
-    def layer(l, carry):
-        flip = lax.rem(l, 2)
-
-        def at(i):
-            return i + flip * (chunks - 1 - 2 * i)
-
-        p = [at(i) for i in (1, 2, 3, 0)]
-        order = [at(i) for i in (2, 1, 0, 3)]
-        started = l > 0
-        last = l == layers - 1
-
-        def arrive(i):
-            @pl.when(started)
-            def _():
-                finish(l - 1, i)
-
-            @pl.when(jnp.logical_not(started))
-            def _():
-                init(i)
-
-        def leave(i):
-            @pl.when(last)
-            def _():
-                finish_last(l, i)
-
-            @pl.when(jnp.logical_not(last))
-            def _():
-                finish(l, i)
-
-        for c in weight_copies(l):
-            c.wait()
-        qkv(l, p[0])
-        arrive(p[2])
-        qkv(l, p[1])
-        arrive(p[3])
-        qkv(l, p[2])
-
-        @pl.when(flip == 0)
-        def _():
-            halo_copies(l)[0].start()
-
-        @pl.when(flip == 1)
-        def _():
-            halo_copies(l)[1].start()
-
-        attend(l, order[0])
-        for c in own_out(l):
-            c.wait()
-        for c in partner_out(l):
-            c.wait_recv()
-        project(l, order[0])
-        qkv(l, p[3])
-
-        @pl.when(flip == 0)
-        def _():
-            halo_copies(l)[1].start()
-
-        @pl.when(flip == 1)
-        def _():
-            halo_copies(l)[0].start()
-
-        attend(l, order[1])
-        project(l, order[1])
-        leave(order[0])
-
-        @pl.when(flip == 0)
-        def _():
-            halo_copies(l)[0].wait_recv()
-
-        @pl.when(flip == 1)
-        def _():
-            halo_copies(l)[1].wait_recv()
-
-        attend(l, order[2])
-        project(l, order[2])
-        leave(order[1])
-
-        @pl.when(flip == 0)
-        def _():
-            halo_copies(l)[1].wait_recv()
-
-        @pl.when(flip == 1)
-        def _():
-            halo_copies(l)[0].wait_recv()
-
-        attend(l, order[3])
-        project(l, order[3])
-        return carry
-
-    init(first[0])
-    init(first[1])
-    lax.fori_loop(0, layers, layer, 0)
-    flip = (layers - 1) % 2
-    for i in (0, 3):
-        finish_last(layers - 1, chunks - 1 - i if flip else i)
+            to = lax.rem(sp + k, n)
+            if b1 == b0 + 1:
+                out_list.append(remote(xo.at[i, :, to], out.at[mine_at, b0 : b0 + 2], out_s.at[i], out_r.at[i], (to, tp)))
+            else:
+                for j, blk in enumerate((b0, b1)):
+                    out_list.append(remote(xo.at[i, j, to], out.at[mine_at, blk], out_s.at[i], out_r.at[i], (to, tp)))
+        return out_list
+
+    def finish_last(i):
+        rows = jnp.dot(swap, updated(i), preferred_element_type=f32)
+        xo[i] = rows.reshape(2, n, half // n, chan).astype(bf16)
+        for c in out_copies(i):
+            c.start()
+        for j, blk in enumerate(units[layers][i]):
+            out[mine_at, blk] = xo[i, j, sp]
+
+    def leave(l, i):
+        if l == layers - 1:
+            finish_last(i)
+        else:
+            finish(l, i)
+
+    def load(l, what):
+        for c in what(l):
+            c.start()
+
+    seen = set()
+
+    def once(*key):
+        fresh = key not in seen
+        seen.add(key)
+        return fresh
+
+    for kind, l, i in steps:
+        if kind == "init":
+            init(i)
+            if l + 1 < layers and once("load", l + 1):
+                load(l + 1, weight_copies)
+                load(l + 1, own_out)
+        elif kind == "relay":
+            relay(l, i)
+        elif kind == "qkv":
+            if once("weights", l):
+                for c in weight_copies(l):
+                    c.wait()
+            qkv(l, i)
+        elif kind == "attend":
+            for blk in units[l + 1][i]:
+                if blk in (0, blocks - 1) and once("halo", l, blk):
+                    halo_copies(l)[0 if blk == 0 else 1].wait_recv()
+            attend(l, i)
+        elif kind == "project":
+            if once("out", l):
+                for c in own_out(l):
+                    c.wait()
+                for c in partner_out(l):
+                    c.wait_recv()
+            project(l, i)
+            if l + 1 < layers and once("load out", l + 1):
+                load(l + 1, partner_out)
+            if l + 2 < layers and once("load", l + 2):
+                load(l + 2, weight_copies)
+                load(l + 2, own_out)
+        else:
+            leave(l, i)
 
     for i in range(chunks):
-        some = out.at[pl.ds(0, n - 1), i]
+        some = xo.at[i, :, pl.ds(0, n - 1)]
         pltpu.make_async_copy(some, some, out_r.at[i]).wait()
-        some = xo.at[i, pl.ds(0, n - 1)]
         pltpu.make_async_copy(some, some, out_s.at[i]).wait()
-        some = xt.at[pl.ds(0, n - 1), i]
-        pltpu.make_async_copy(some, some, in_s.at[i]).wait()
+        if i >= chunks - 2:
+            sent_in(i)
     for l in range(layers):
         for c in partner_out(l) + halo_copies(l):
             c.wait_send()
         for i in range(chunks):
-            for c in ag_copies(l, i) + [relay_copy(l, i), mx_copy(l, i), rs_copy(l, i)]:
+            moved = ag_copies(l, i) + [relay_copy(l, i)] if l == 0 else partner_copies(l, i)
+            moved += [mx_copy(l, i)] + [rs_copy(l, i, o) for o in range(1 if l == layers - 1 else 2)]
+            for c in moved:
                 c.wait_send()
 
 
@@ -478,30 +612,32 @@
     heads = rel_bias.shape[1]
     chunks = columns // n // WIN_C
     bf16, f32 = jnp.bfloat16, jnp.float32
-    turned = jnp.transpose(token_grid, (0, 2, 1)).reshape(n, chunks, WIN_C, chan)
+    turned = jnp.transpose(token_grid, (0, 2, 1)).reshape(n, 2 * chunks, WIN_C // 2, chan)
     tok = WIN_C * WIN_R
     half = tok // 2
-    cfg = (layers, n, chunks, WIN_C, chan, heads, width)
+    same = tuple(range(chunks))
+    orders = [same[:-2] + (same[-1], same[-2])] * (layers - 1) + [same]
+    cfg = (layers, n, chunks, WIN_C, chan, heads, width, plan(layers, 2 * chunks, same, orders))
     vmem = pl.BlockSpec(memory_space=pltpu.VMEM)
     hbm = pl.BlockSpec(memory_space=pl.ANY)
     dma = pltpu.SemaphoreType.DMA
     out = pl.pallas_call(
         functools.partial(mega_kernel, cfg),
-        out_shape=jax.ShapeDtypeStruct((n, chunks, WIN_C, chan), bf16),
+        out_shape=jax.ShapeDtypeStruct((n, 2 * chunks, WIN_C // 2, chan), bf16),
         in_specs=[vmem, vmem, vmem, hbm, hbm, hbm, hbm],
         out_specs=vmem,
         scratch_shapes=[
             pltpu.VMEM((layers, 3, width, chan), bf16),
             pltpu.VMEM((layers, 2, 2, chan, chan), bf16),
             pltpu.VMEM((layers, width // chan, chunks, tok, chan), bf16),
-            pltpu.VMEM((chunks, n, WIN_C, chan), bf16),
-            pltpu.VMEM((chunks, n, WIN_C, chan), bf16),
+            pltpu.VMEM((chunks, 2, n, WIN_C // 2, chan), bf16),
+            pltpu.VMEM((chunks, 2, n, WIN_C // 2, chan), bf16),
             pltpu.VMEM((tok, width), bf16),
-            pltpu.VMEM((chunks, tok, chan), bf16),
+            pltpu.VMEM((2 * chunks, half, chan), bf16),
             pltpu.VMEM((layers, 2, 2 * chunks + 2, half, chan), bf16),
             pltpu.VMEM((layers, 2, chunks, tok, chan), bf16),
-            pltpu.VMEM((layers, chunks, tok, chan), bf16),
-            pltpu.VMEM((layers, chunks, tok, chan), bf16),
+            pltpu.VMEM((layers, chunks, 2, tok, chan), bf16),
+            pltpu.VMEM((layers, chunks, 2, tok, chan), bf16),
             pltpu.VMEM((chunks, tok, chan), f32),
             pltpu.VMEM((layers, heads, tok, 2 * tok), f32),
             pltpu.VMEM((layers * heads * WIN_R, LANES), f32),
@@ -517,8 +653,8 @@
             dma((layers, 2)),
             dma((layers, chunks)),
             dma((layers, chunks)),
-            dma((layers, chunks)),
-            dma((layers, chunks)),
+            dma((layers, chunks, 2)),
+            dma((layers, chunks, 2)),
             dma((chunks,)),
             dma((chunks,)),
         ],

time: 112 us -> 104 us (0.929)
  Pallas kernels: 107 us -> 98.2 us
    pallas_call x1, Pallas kernels: 107 us -> 98.2 us  [fused_body(): pl.pallas_call(functools.partial(mega_kernel, cfg), out_shape=jax.ShapeDt...]
where the time goes in v3:
time: 104 us
  Pallas kernels  98.2 us (94%)
  local copies, waits for them, and re-layouts  5.42 us (5%)
    pallas_call x1, Pallas kernels, fused_body(): pl.pallas_call(functools.partial(mega_kernel, cfg), out_shape=jax.ShapeDt...  98.2 us

profile of v3, /device:TPU:0, one launch (start us, length us, event | category | flops | bytes accessed | tf_op | source)
XLA Modules:
  0.0 103.7 jit_solution(7652731905296838644)
XLA Ops:
  0.0 1.3 %reshape.20.refs_1_ = f32[3,1,2048]{2,1,0:T(1,128)} reshape(bf16[3,2048]{1,0:T(4,128)(2,1)} %param.8) | data formatting | bytes 36864 | tf_op jit(solution)/shard_map/reshape | solution.py:665
  1.3 2.0 %copy.8 = bf16[1,512,512]{2,1,0:T(8,128)(2,1)} copy(bf16[1,512,512]{1,2,0:T(8,128)(2,1)} %bitcast.7) | data formatting | bytes 1048576 | tf_op jit(solution)/shard_map/transpose | solution.py:615
  3.4 98.2 %grid_attention.1 = bf16[8,8,8,512]{3,2,1,0:T(8,128)(2,1)} custom-call(bf16[8,8,8,512]{3,2,1,0:T(8,128)(2,1)} %bitcast.6, f32[3,1,2048]{2,1,0:T(1,128)} %reshape.20.refs_1_, f32[192,16]{1,0:T(8,128)} %bitcast.8, bf16[3,2048,512]{2,1,0:T(8,128)(2,1)} %refs_3_.1, bf16[3,2048,512]{2,1,0:T(8,128)(2,1)} %refs_4_.1, bf16[3,2048,512]{2,1,0:T(8,128)(2,1)} %refs_5_.1, ...), custom_call_target="tpu_custom_call" | custom-call | tf_op jit(solution)/shard_map/grid_attention/pallas_call | solution.py:624
  101.6 2.0 %copy.9 = bf16[1,512,512]{1,2,0:T(8,128)(2,1)} copy(bf16[1,512,512]{2,1,0:T(8,128)(2,1)} %bitcast.5) | data formatting | bytes 1048576 | tf_op jit(solution)/shard_map/reshape | solution.py:666

commit v4 on v3

--- a/solution.py
+++ b/solution.py
@@ -14,6 +14,7 @@
 LANES = 128
 NEG = -1e30
 MESH = pl.DeviceIdType.MESH
+ORDERS = ((0, 1, 3, 2), (0, 2, 3, 1), (0, 3, 1, 2), (0, 3, 1, 2))
 
 
 def attention_kernel(rows, cols, q_ref, k_ref, v_ref, kh_ref, vh_ref, base_ref, o_ref, tile_ref):
@@ -176,11 +177,11 @@
 
 
 def plan(layers, blocks, starts, orders):
-    link, hop, near, mixed, halo_link, halo_hop = 2.82, 1.8, 1.45, 1.4, 2.8, 2.2
+    link, hop, near, mixed, halo_link, halo_hop = 2.82, 1.8, 2.0, 1.6, 2.8, 3.0
     odd, even = unit_pairs(blocks)
     units = [odd if l % 2 == 0 else even for l in range(layers + 1)]
     count = len(odd)
-    gathered = [starts] + orders
+    gathered = [starts] + list(orders)
 
     def needs(l, i):
         wanted, sides = set(), []
@@ -266,7 +267,7 @@
     layers, n, chunks, ccols, chan, heads, width, steps = cfg
     (xt, gain, bias, wq, wk, wv, wo, out,
      w_v, wo_v, xg, xin, xo, sc, q_s, kv, mx, rs_s, rs_r, pre, tile, wide,
-     w_sem, wol_sem, wos_sem, wor_sem, in_s, in_r, ags, agr, hs, hr, ms, mr, rss, rsr, out_s, out_r) = refs
+     w_sem, wol_sem, wor_sem, in_s, in_r, far_r, near_r, hr, mr, rsr, sent, out_r) = refs
     f32, bf16 = jnp.float32, jnp.bfloat16
     tok = ccols * WIN_R
     half = tok // 2
@@ -288,10 +289,17 @@
     mine_at = place(sp)
     right, left = holder(lax.rem(mine_at + 1, n)), holder(lax.rem(mine_at + n - 1, n))
 
+    wo_sent, ag_sent, pair_sent, halo_sent, mx_sent, sum_sent, last_sent, out_sent = (sent.at[k] for k in range(8))
+
+    def wait_for(some, sem):
+        pltpu.make_async_copy(some, some, sem).wait()
+
     def remote(src, dst, ssem, rsem, dev):
         return pltpu.make_async_remote_copy(
             src_ref=src, dst_ref=dst, send_sem=ssem, recv_sem=rsem, device_id=dev, device_id_type=MESH
         )
+
+    far_first = sorted(range(1, n), key=lambda k: -min(k, n - k))
 
     bar = pltpu.get_barrier_semaphore()
     for k in range(1, n):
@@ -306,7 +314,7 @@
 
     def sends_in(i):
         (b0, b1), out = odd[i], []
-        for k in range(1, n):
+        for k in far_first:
             to = lax.rem(sp + k, n)
             if b1 == b0 + 1:
                 out.append(remote(xt.at[place(to), b0 : b0 + 2], xin.at[i, :, sp], in_s.at[i], in_r.at[i], (to, tp)))
@@ -315,26 +323,29 @@
                     out.append(remote(xt.at[place(to), blk], xin.at[i, j, sp], in_s.at[i], in_r.at[i], (to, tp)))
         return out
 
+    def own_inputs(i):
+        return [pltpu.make_async_copy(xt.at[mine_at, blk], xin.at[i, j, sp], in_r.at[i]) for j, blk in enumerate(odd[i])]
+
     def sent_in(i):
-        some = xin.at[i, :, pl.ds(0, n - 1)]
-        pltpu.make_async_copy(some, some, in_s.at[i]).wait()
-
-    for i in range(2):
-        for c in sends_in(i):
+        wait_for(xin.at[i, :, pl.ds(0, n - 1)], in_s.at[i])
+
+    starts = [i for kind, _, i in steps if kind == "init"]
+    for i in starts[:2]:
+        for c in own_inputs(i) + sends_in(i):
             c.start()
 
     def weight_copies(l):
-        return [pltpu.make_async_copy(w.at[l], w_v.at[l, m], w_sem.at[l, m]) for m, w in enumerate((wk, wv, wq))]
+        return [pltpu.make_async_copy(w.at[l], w_v.at[l, m], w_sem.at[l]) for m, w in enumerate((wk, wv, wq))]
 
     def cols_of(c, o):
         return pl.ds(pl.multiple_of((o * 2 + c) * chan, 128), chan)
 
     def own_out(l):
-        return [pltpu.make_async_copy(wo.at[l, :, cols_of(core, o)], wo_v.at[l, core, o], wol_sem.at[l, o]) for o in range(2)]
+        return [pltpu.make_async_copy(wo.at[l, :, cols_of(core, o)], wo_v.at[l, core, o], wol_sem.at[l]) for o in range(2)]
 
     def partner_out(l):
         return [
-            remote(wo.at[l, :, cols_of(1 - core, o)], wo_v.at[l, core, o], wos_sem.at[l, o], wor_sem.at[l, o], (sp, partner))
+            remote(wo.at[l, :, cols_of(1 - core, o)], wo_v.at[l, core, o], wo_sent, wor_sem.at[l], (sp, partner))
             for o in range(2)
         ]
 
@@ -363,9 +374,9 @@
 
     lax.fori_loop(0, layers * heads, build, 0)
 
-    for i in range(2, chunks):
-        sent_in(i - 2)
-        for c in sends_in(i):
+    for was, i in zip(starts, starts[2:]):
+        sent_in(was)
+        for c in own_inputs(i) + sends_in(i):
             c.start()
 
     a = lax.broadcasted_iota(jnp.int32, (tok, tok), 0)
@@ -378,13 +389,13 @@
     def ag_copies(l, i):
         own = xg.at[l, tp, i]
         return [
-            remote(own, own, ags.at[l, i, 0], agr.at[l, i, 0], (sp, ypeer)),
-            remote(own, own, ags.at[l, i, 1], agr.at[l, i, 1], (sp, partner)),
+            remote(own, own, ag_sent, far_r.at[i], (sp, ypeer)),
+            remote(own, own, ag_sent, near_r.at[l, i], (sp, partner)),
         ]
 
     def relay_copy(l, i):
         slot = xg.at[l, ypeer, i]
-        return remote(slot, slot, ags.at[l, i, 2], agr.at[l, i, 2], (sp, partner))
+        return remote(slot, slot, ag_sent, near_r.at[l, i], (sp, partner))
 
     def ag_send(l, i):
         for c in ag_copies(l, i):
@@ -396,30 +407,21 @@
 
     def partner_copies(l, i):
         slots = [xg.at[l, 2 * o + core, i] for o in range(2)]
-        return [remote(slots[o], slots[o], ags.at[l, i, o], agr.at[l, i, o], (sp, partner)) for o in range(2)]
+        return [remote(slots[o], slots[o], pair_sent, near_r.at[l, i], (sp, partner)) for o in range(2)]
 
     def ag_recv(l, i):
-        if l == 0:
-            ag_copies(l, i)[1].wait_recv()
-            relay_copy(l, i).wait_recv()
-        else:
-            for c in partner_copies(l, i):
-                c.wait_recv()
+        wait_for(xg.at[l, pl.ds(0, 2), i], near_r.at[l, i])
 
     def init(i):
-        b0, b1 = odd[i]
-        for j, blk in enumerate((b0, b1)):
-            xin[i, j, sp] = xt[mine_at, blk]
-        some = xin.at[i, :, pl.ds(0, n - 1)]
-        pltpu.make_async_copy(some, some, in_r.at[i]).wait()
+        wait_for(xin.at[i], in_r.at[i])
         raw = xin[i].astype(f32).reshape(tok, chan).astype(bf16)
         xg[0, tp, i] = jnp.dot(swap, raw, preferred_element_type=f32).astype(bf16)
         ag_send(0, i)
 
     def halo_copies(l):
         return [
-            remote(kv.at[l, :, 2 * chunks], kv.at[l, :, 0], hs.at[l, 0], hr.at[l, 0], (right, tp)),
-            remote(kv.at[l, :, 1], kv.at[l, :, 2 * chunks + 1], hs.at[l, 1], hr.at[l, 1], (left, tp)),
+            remote(kv.at[l, :, 2 * chunks], kv.at[l, :, 0], halo_sent, hr.at[l, 0], (right, tp)),
+            remote(kv.at[l, :, 1], kv.at[l, :, 2 * chunks + 1], halo_sent, hr.at[l, 1], (left, tp)),
         ]
 
     def qkv(l, i):
@@ -428,7 +430,7 @@
         for s in range(width // chan):
             raw = xg[l, s, i].astype(f32)
             total = total + jnp.sum(raw * raw, axis=1, keepdims=True)
-            sc[:, s * chan : (s + 1) * chan] = (raw * gain[l, :, s * chan : (s + 1) * chan]).astype(bf16)
+            sc[:, s * chan : (s + 1) * chan] = (raw * gain[l : l + 1, s * chan : (s + 1) * chan].astype(f32)).astype(bf16)
         inverse = lax.rsqrt(total / width + EPS)
         x = sc[...]
         for m in range(2):
@@ -447,7 +449,7 @@
 
     def mx_copy(l, i):
         slot = mx.at[l, core, i]
-        return remote(slot, slot, ms.at[l, i], mr.at[l, i], (sp, partner))
+        return remote(slot, slot, mx_sent, mr.at[l, i], (sp, partner))
 
     def window(l, q0, qn, k0, t0, out_at):
         rows = qn * half
@@ -480,7 +482,8 @@
         mx_copy(l, i).start()
 
     def rs_copy(l, i, o):
-        return remote(rs_s.at[l, i, o], rs_r.at[l, i, o], rss.at[l, i, o], rsr.at[l, i, o], (sp, ypeer))
+        done = last_sent if l == layers - 1 else sum_sent
+        return remote(rs_s.at[l, i, o], rs_r.at[l, i, o], done, rsr.at[l, i, o], (sp, ypeer))
 
     def old(l, i, slot):
         parts = []
@@ -522,22 +525,28 @@
 
     def out_copies(i):
         (b0, b1), out_list = units[layers][i], []
-        for k in range(1, n):
+        for k in far_first:
             to = lax.rem(sp + k, n)
             if b1 == b0 + 1:
-                out_list.append(remote(xo.at[i, :, to], out.at[mine_at, b0 : b0 + 2], out_s.at[i], out_r.at[i], (to, tp)))
+                out_list.append(remote(xo.at[i, :, to], out.at[mine_at, b0 : b0 + 2], out_sent, out_r.at[0], (to, tp)))
             else:
                 for j, blk in enumerate((b0, b1)):
-                    out_list.append(remote(xo.at[i, j, to], out.at[mine_at, blk], out_s.at[i], out_r.at[i], (to, tp)))
+                    out_list.append(remote(xo.at[i, j, to], out.at[mine_at, blk], out_sent, out_r.at[0], (to, tp)))
         return out_list
+
+    def own_results(i):
+        return [
+            pltpu.make_async_copy(xo.at[i, j, sp], out.at[mine_at, blk], out_r.at[0])
+            for j, blk in enumerate(units[layers][i])
+        ]
 
     def finish_last(i):
         rows = jnp.dot(swap, updated(i), preferred_element_type=f32)
         xo[i] = rows.reshape(2, n, half // n, chan).astype(bf16)
         for c in out_copies(i):
             c.start()
-        for j, blk in enumerate(units[layers][i]):
-            out[mine_at, blk] = xo[i, j, sp]
+        for c in own_results(i):
+            c.start()
 
     def leave(l, i):
         if l == layers - 1:
@@ -566,8 +575,7 @@
             relay(l, i)
         elif kind == "qkv":
             if once("weights", l):
-                for c in weight_copies(l):
-                    c.wait()
+                wait_for(w_v.at[l], w_sem.at[l])
             qkv(l, i)
         elif kind == "attend":
             for blk in units[l + 1][i]:
@@ -576,10 +584,8 @@
             attend(l, i)
         elif kind == "project":
             if once("out", l):
-                for c in own_out(l):
-                    c.wait()
-                for c in partner_out(l):
-                    c.wait_recv()
+                wait_for(wo_v.at[l, core], wol_sem.at[l])
+                wait_for(wo_v.at[l, 1 - core], wor_sem.at[l])
             project(l, i)
             if l + 1 < layers and once("load out", l + 1):
                 load(l + 1, partner_out)
@@ -589,20 +595,17 @@
         else:
             leave(l, i)
 
-    for i in range(chunks):
-        some = xo.at[i, :, pl.ds(0, n - 1)]
-        pltpu.make_async_copy(some, some, out_r.at[i]).wait()
-        pltpu.make_async_copy(some, some, out_s.at[i]).wait()
-        if i >= chunks - 2:
-            sent_in(i)
-    for l in range(layers):
-        for c in partner_out(l) + halo_copies(l):
-            c.wait_send()
-        for i in range(chunks):
-            moved = ag_copies(l, i) + [relay_copy(l, i)] if l == 0 else partner_copies(l, i)
-            moved += [mx_copy(l, i)] + [rs_copy(l, i, o) for o in range(1 if l == layers - 1 else 2)]
-            for c in moved:
-                c.wait_send()
+    wait_for(xo, out_r.at[0])
+    wait_for(xo.at[:, :, pl.ds(0, n - 1)], out_sent)
+    for i in starts[2:]:
+        sent_in(i)
+    wait_for(wo_v.at[:, 0], wo_sent)
+    wait_for(xg.at[0, pl.ds(0, 3)], ag_sent)
+    wait_for(xg.at[pl.ds(1, layers - 1), pl.ds(0, 2)], pair_sent)
+    wait_for(kv.at[:, :, pl.ds(0, 2)], halo_sent)
+    wait_for(mx.at[:, 0], mx_sent)
+    wait_for(rs_s.at[pl.ds(0, layers - 1)], sum_sent)
+    wait_for(rs_s.at[layers - 1, :, 0], last_sent)
 
 
 def fused_body(token_grid, norm_gain, w_query, w_key, w_value, w_out, rel_bias):
@@ -615,17 +618,14 @@
     turned = jnp.transpose(token_grid, (0, 2, 1)).reshape(n, 2 * chunks, WIN_C // 2, chan)
     tok = WIN_C * WIN_R
     half = tok // 2
-    same = tuple(range(chunks))
-    orders = [same[:-2] + (same[-1], same[-2])] * (layers - 1) + [same]
-    cfg = (layers, n, chunks, WIN_C, chan, heads, width, plan(layers, 2 * chunks, same, orders))
-    vmem = pl.BlockSpec(memory_space=pltpu.VMEM)
-    hbm = pl.BlockSpec(memory_space=pl.ANY)
+    cfg = (layers, n, chunks, WIN_C, chan, heads, width, plan(layers, 2 * chunks, ORDERS[0], ORDERS[1:]))
+    hbm, vmem = pl.BlockSpec(memory_space=pl.ANY), pl.BlockSpec(memory_space=pltpu.VMEM)
     dma = pltpu.SemaphoreType.DMA
     out = pl.pallas_call(
         functools.partial(mega_kernel, cfg),
         out_shape=jax.ShapeDtypeStruct((n, 2 * chunks, WIN_C // 2, chan), bf16),
-        in_specs=[vmem, vmem, vmem, hbm, hbm, hbm, hbm],
-        out_specs=vmem,
+        in_specs=[hbm, vmem, vmem] + [hbm] * 4,
+        out_specs=hbm,
         scratch_shapes=[
             pltpu.VMEM((layers, 3, width, chan), bf16),
             pltpu.VMEM((layers, 2, 2, chan, chan), bf16),
@@ -641,28 +641,24 @@
             pltpu.VMEM((chunks, tok, chan), f32),
             pltpu.VMEM((layers, heads, tok, 2 * tok), f32),
             pltpu.VMEM((layers * heads * WIN_R, LANES), f32),
-            dma((layers, 3)),
-            dma((layers, 2)),
-            dma((layers, 2)),
-            dma((layers, 2)),
+            dma((layers,)),
+            dma((layers,)),
+            dma((layers,)),
             dma((chunks,)),
             dma((chunks,)),
-            dma((layers, chunks, 3)),
-            dma((layers, chunks, 3)),
-            dma((layers, 2)),
+            dma((chunks,)),
+            dma((layers, chunks)),
             dma((layers, 2)),
             dma((layers, chunks)),
-            dma((layers, chunks)),
             dma((layers, chunks, 2)),
-            dma((layers, chunks, 2)),
-            dma((chunks,)),
-            dma((chunks,)),
+            dma((8,)),
+            dma((1,)),
         ],
         compiler_params=pltpu.CompilerParams(
-            collective_id=0, has_side_effects=True, vmem_limit_bytes=60 * 1024 * 1024
+            collective_id=0, has_side_effects=True, vmem_limit_bytes=52 * 1024 * 1024
         ),
         name="grid_attention",
-    )(turned, norm_gain.astype(f32).reshape(layers, 1, width), rel_bias.reshape(-1, WIN_C), w_query, w_key, w_value, w_out)
+    )(turned, norm_gain, rel_bias.reshape(-1, WIN_C), w_query, w_key, w_value, w_out)
     return jnp.transpose(out.reshape(rows_dev, columns, chan), (0, 2, 1))
 
 
@@ -682,7 +678,8 @@
     def run(token_grid, *rest):
         rows, _, columns = token_grid.shape
         n = mesh.shape["sp"]
-        whole = rows == n == WIN_R and columns == 4 * WIN_C * n and mesh.shape["tp"] == 4
+        whole = rows == n == WIN_R and columns == len(ORDERS[0]) * WIN_C * n and mesh.shape["tp"] == 4
+        whole = whole and rest[0].shape[0] == len(ORDERS) - 1
         return sharded(fused_body if whole else body)(token_grid, *rest)
 
     return run

time: 104 us -> 99.5 us (0.957)
  Pallas kernels: 98.2 us -> 95.4 us
  local copies, waits for them, and re-layouts: 5.42 us -> 3.86 us
    pallas_call x1, Pallas kernels: 98.2 us -> 95.4 us  [fused_body(): pl.pallas_call(functools.partial(mega_kernel, cfg), out_shape=jax.ShapeDt...]
    unnamed x0 -> x4, local copies, waits for them, and re-layouts: none -> 1.6 us
    reshape x1 -> x0, local copies, waits for them, and re-layouts: 1.33 us -> none  [fused_body(): norm_gain.astype(f32).reshape(layers, 1, width)]
    reshape x1, local copies, waits for them, and re-layouts: 2.05 us -> 1 us  [fused_body(): return jnp.transpose(out.reshape(rows_dev, columns, chan), (0, 2, 1))]
where the time goes in v4:
time: 99.5 us; the launch traced here: 99.3 us
  Pallas kernels  95.4 us (96%)
  local copies, waits for them, and re-layouts  3.86 us (4%)
    pallas_call x1, Pallas kernels, fused_body(): pl.pallas_call(functools.partial(mega_kernel, cfg), out_shape=jax.ShapeDt...  95.4 us

profile of v4, /device:TPU:0, one launch (start us, length us, event | category | flops | bytes accessed | tf_op | source)
XLA Modules:
  0.0 99.3 jit_solution(7458580560899174607)
XLA Ops:
  0.0 1.3 %copy.8 = bf16[1,512,512]{2,1,0:T(8,128)(2,1)S(1)} copy(bf16[1,512,512]{1,2,0:T(8,128)(2,1)} %bitcast.8) | data formatting | bytes 1048576 | tf_op jit(solution)/shard_map/transpose | solution.py:618
  1.3 0.0 copy-start
  1.3 0.9 copy-done
  2.2 0.0 copy-start.1
  2.2 0.7 copy-done.1
  2.9 95.4 %grid_attention.1 = bf16[8,8,8,512]{3,2,1,0:T(8,128)(2,1)S(1)} custom-call(bf16[8,8,8,512]{3,2,1,0:T(8,128)(2,1)S(1)} %bitcast.6, bf16[3,2048]{1,0:T(4,128)(2,1)S(1)} %copy-done.1, f32[192,16]{1,0:T(8,128)S(1)} %bitcast.7, bf16[3,2048,512]{2,1,0:T(8,128)(2,1)} %refs_3_.1, bf16[3,2048,512]{2,1,0:T(8,128)(2,1)} %refs_4_.1, bf16[3,2048,512]{2,1,0:T(8,128)(2,1)} %refs_5_.1, ...), custom_call_target="tpu_custom_call" | custom-call | tf_op jit(solution)/shard_map/grid_attention/pallas_call | solution.py:624
  98.3 1.0 %copy.9 = bf16[1,512,512]{1,2,0:T(8,128)(2,1)} copy(bf16[1,512,512]{2,1,0:T(8,128)(2,1)S(1)} %bitcast.5) | data formatting | bytes 1048576 | tf_op jit(solution)/shard_map/reshape | solution.py:662
Async XLA Ops:
  1.3 0.9 copy-start
  2.2 0.7 copy-start.1

commit v5 on v4

--- a/solution.py
+++ b/solution.py
@@ -14,7 +14,7 @@
 LANES = 128
 NEG = -1e30
 MESH = pl.DeviceIdType.MESH
-ORDERS = ((0, 1, 3, 2), (0, 2, 3, 1), (0, 3, 1, 2), (0, 3, 1, 2))
+ORDERS = ((3, 0, 1, 2), (3, 2, 0, 1), (0, 3, 2, 1), (2, 3, 0, 1))
 
 
 def attention_kernel(rows, cols, q_ref, k_ref, v_ref, kh_ref, vh_ref, base_ref, o_ref, tile_ref):
@@ -177,7 +177,8 @@
 
 
 def plan(layers, blocks, starts, orders):
-    link, hop, near, mixed, halo_link, halo_hop = 2.82, 1.8, 2.0, 1.6, 2.8, 3.0
+    link, hop, near, mixed, halo_link, halo_hop = 2.82, 2.0, 2.6, 1.5, 2.8, 2.8
+    arrival = (4.6, 8.6, 11.0, 13.5)
     odd, even = unit_pairs(blocks)
     units = [odd if l % 2 == 0 else even for l in range(layers + 1)]
     count = len(odd)
@@ -207,7 +208,7 @@
     while True:
         ready = []
         if first < count:
-            ready.append((4.5 + 2.7 * first, 0, "init", 0, starts[first]))
+            ready.append((arrival[first], 0, "init", 0, starts[first]))
         for l in range(layers):
             def step(kind, order):
                 return order[at[kind][l]] if at[kind][l] < count else None
@@ -232,7 +233,8 @@
         if not ready:
             return steps
         can = [r for r in ready if r[0] <= now]
-        when, _, kind, l, i = min(can, key=lambda r: r[1:]) if can else min(ready)
+        idle = [r for r in ready if r[2] == "project" and wire <= max(now, r[0]) and r[0] <= now + mixed]
+        when, _, kind, l, i = min(idle) if idle else min(can, key=lambda r: r[1:]) if can else min(ready)
         now = max(now, when)
         steps.append((kind, l, i))
         if kind == "init":
@@ -568,7 +570,7 @@
     for kind, l, i in steps:
         if kind == "init":
             init(i)
-            if l + 1 < layers and once("load", l + 1):
+            if i == starts[-1] and l + 1 < layers and once("load", l + 1):
                 load(l + 1, weight_copies)
                 load(l + 1, own_out)
         elif kind == "relay":

time: 99.5 us -> 98.8 us (level)
  no operation moved by 1% of the time
where the time goes in v5:
time: 98.8 us; the launch traced here: 98.6 us
  Pallas kernels  94.7 us (96%)
  local copies, waits for them, and re-layouts  3.86 us (4%)
    pallas_call x1, Pallas kernels, fused_body(): pl.pallas_call(functools.partial(mega_kernel, cfg), out_shape=jax.ShapeDt...  94.7 us

profile of v5, /device:TPU:0, one launch (start us, length us, event | category | flops | bytes accessed | tf_op | source)
XLA Modules:
  0.0 98.6 jit_solution(12949542875338291216)
XLA Ops:
  0.0 1.3 %copy.8 = bf16[1,512,512]{2,1,0:T(8,128)(2,1)S(1)} copy(bf16[1,512,512]{1,2,0:T(8,128)(2,1)} %bitcast.8) | data formatting | bytes 1048576 | tf_op jit(solution)/shard_map/transpose | solution.py:620
  1.3 0.0 copy-start
  1.3 0.9 copy-done
  2.2 0.0 copy-start.1
  2.2 0.7 copy-done.1
  2.9 94.7 %grid_attention.1 = bf16[8,8,8,512]{3,2,1,0:T(8,128)(2,1)S(1)} custom-call(bf16[8,8,8,512]{3,2,1,0:T(8,128)(2,1)S(1)} %bitcast.6, bf16[3,2048]{1,0:T(4,128)(2,1)S(1)} %copy-done.1, f32[192,16]{1,0:T(8,128)S(1)} %bitcast.7, bf16[3,2048,512]{2,1,0:T(8,128)(2,1)} %refs_3_.1, bf16[3,2048,512]{2,1,0:T(8,128)(2,1)} %refs_4_.1, bf16[3,2048,512]{2,1,0:T(8,128)(2,1)} %refs_5_.1, ...), custom_call_target="tpu_custom_call" | custom-call | tf_op jit(solution)/shard_map/grid_attention/pallas_call | solution.py:626
  97.6 1.0 %copy.9 = bf16[1,512,512]{1,2,0:T(8,128)(2,1)} copy(bf16[1,512,512]{2,1,0:T(8,128)(2,1)S(1)} %bitcast.5) | data formatting | bytes 1048576 | tf_op jit(solution)/shard_map/reshape | solution.py:664
Async XLA Ops:
  1.3 0.9 copy-start
  2.2 0.7 copy-start.1
